TPU v7x, 512 devices: a whole 4x4x16 slice. The times are simulated.
512 devices in a mesh: sp: 16 (over y, x), tp: 32 (over z, core).
Axes of the slice: x: 4, y: 4, z: 16, core: 2. Of those that a mesh axis runs over, the one named last changes fastest.
Arguments:
- stream: bfloat16 [8192, 4096], P('sp', 'tp'), may hold values from -6 to 6
- gain_first: bfloat16 [4096], P('tp'), may hold values from 0.099609375 to 1.8984375
- query_first: bfloat16 [4096, 4096], P('sp', 'tp'), may hold values from -0.09375 to 0.09375
- key_first: bfloat16 [4096, 4096], P('sp', 'tp'), may hold values from -0.09375 to 0.09375
- value_first: bfloat16 [4096, 4096], P('sp', 'tp'), may hold values from -0.09375 to 0.09375
- offset_first: float32 [32, 15, 31], P('tp'), may hold values from -4 to 254
- gain_second: bfloat16 [4096], P('tp'), may hold values from 0.099609375 to 1.8984375
- query_second: bfloat16 [4096, 4096], P('sp', 'tp'), may hold values from -0.09375 to 0.09375
- key_second: bfloat16 [4096, 4096], P('sp', 'tp'), may hold values from -0.09375 to 0.09375
- value_second: bfloat16 [4096, 4096], P('sp', 'tp'), may hold values from -0.09375 to 0.09375
- offset_second: float32 [32, 15, 31], P('tp'), may hold values from -4 to 254
Outputs:
- result: bfloat16 [8192, 4096], P('sp', 'tp')
All inputs are finite; a program needn't handle non-finite values.
Results may differ from a plain program's by a relative error of at most 0.008.
Values may be sent and summed in bfloat16 or wider, within the bound.
A program may use at most 64 MiB of HBM per device.

v0:
```python
import jax
import jax.numpy as jnp
import numpy as np
from jax import lax
from jax.sharding import PartitionSpec as P

GRID_W = 64


epsilon = 1e-06


def turned_gather(arrays, axis, dims):
    turned = [jnp.moveaxis(a, dim, 0) for a, dim in zip(arrays, dims)]
    both = jnp.concatenate([t.reshape(len(t), -1) for t in turned], axis=1)
    filled, at, gathered = (lax.all_gather(both, axis, axis=0, tiled=True), 0, [])
    for t, dim in zip(turned, dims):
        section = filled[:, at : at + t[0].size].reshape(-1, *t.shape[1:])
        gathered.append(jnp.moveaxis(section, 0, dim))
        at += t[0].size
    return tuple(gathered)


def padded_2(block, sides, width):
    for axis, dim in sides:
        count = lax.axis_size(axis)
        forward = [(i, i + 1) for i in range(count - 1)]
        backward = [(target, source) for source, target in forward]
        low = lax.ppermute(
            lax.slice_in_dim(block, block.shape[dim] - width, None, axis=dim), axis, forward
        )
        high = lax.ppermute(lax.slice_in_dim(block, 0, width, axis=dim), axis, backward)
        block = jnp.concatenate([low, block, high], axis=dim)
    return block


def sent_together(arrays, axis, dim, along):
    ends, at = ([], 0)
    for a in arrays[:-1]:
        at += a.shape[along]
        ends.append(at)
    both = jnp.concatenate(arrays, axis=along)
    return tuple(jnp.split(lax.all_gather(both, axis, axis=dim, tiled=True), ends, axis=along))


def attend(query, keys, values, table, row_start, total_rows):
    rows_here, width, heads, head_size = query.shape
    blocks = width // 16
    query_cols = np.arange(width).reshape(blocks, 16)
    window_start = np.clip(query_cols - 8, 0, width - 16)
    key_cols = np.clip(np.arange(blocks) * 16 - 8, 0, width - 32)[:, None] + np.arange(32)
    column_ok = (key_cols[:, None, :] >= window_start[:, :, None]) & (
        key_cols[:, None, :] < window_start[:, :, None] + 16
    )
    column_offset = np.clip(key_cols[:, None, :] - query_cols[:, :, None] + 15, 0, 30)
    column_bias = table[:, :, column_offset]
    mask = jnp.asarray(column_ok)[None, :, :, None, :]
    factor = head_size ** (-0.5)

    def one_row(index):
        grid_row = row_start + index
        first = jnp.clip(grid_row - 4, 0, total_rows - 8)
        local = first - row_start + 4
        key_block = lax.dynamic_slice_in_dim(keys, local, 8, 0)[:, key_cols]
        value_block = lax.dynamic_slice_in_dim(values, local, 8, 0)[:, key_cols]
        query_row = lax.dynamic_index_in_dim(query, index, 0, keepdims=False).reshape(
            blocks, 16, heads, head_size
        )
        scores = (
            jnp.einsum(
                "jqhe,mjkhe->hjqmk", query_row, key_block, preferred_element_type=jnp.float32
            )
            * factor
        )
        row_offset = first + jnp.arange(8, dtype=jnp.int32) - grid_row + 7
        row_bias = jnp.transpose(jnp.take(column_bias, row_offset, axis=1), (0, 2, 3, 1, 4))
        scores = jnp.where(mask, scores + row_bias, -1e30)
        weight = jax.nn.softmax(scores.reshape(heads, blocks, 16, 256), axis=-1)
        rounded = weight.astype(jnp.bfloat16).reshape(heads, blocks, 16, 8, 32)
        output = jnp.einsum(
            "hjqmk,mjkhe->jqhe", rounded, value_block, preferred_element_type=jnp.float32
        )
        return output.reshape(width, heads * head_size)

    return jax.vmap(one_row)(jnp.arange(rows_here, dtype=jnp.int32))


def layer(stream, gain, table, whole_weights):
    tokens_dev, local_width = stream.shape
    widened = stream.astype(jnp.float32)
    full_rows, full_gain = turned_gather((stream, gain), "tp", (1, 0))
    full_wide = full_rows.astype(jnp.float32)
    mean_square = jnp.mean(full_wide * full_wide, axis=-1, keepdims=True)
    normed = (full_wide * lax.rsqrt(mean_square + epsilon) * full_gain.astype(jnp.float32)).astype(
        jnp.bfloat16
    )
    query = jnp.dot(normed, whole_weights[0], preferred_element_type=jnp.float32)
    key_part = jnp.dot(normed, whole_weights[1], preferred_element_type=jnp.float32)
    value_part = jnp.dot(normed, whole_weights[2], preferred_element_type=jnp.float32)
    heads_dev = table.shape[0]
    rows_dev = tokens_dev // GRID_W
    shape = (rows_dev, GRID_W, heads_dev, local_width // heads_dev)
    query = query.astype(jnp.bfloat16).reshape(shape)
    paired = jnp.stack(
        [
            key_part.astype(jnp.bfloat16).reshape(shape),
            value_part.astype(jnp.bfloat16).reshape(shape),
        ]
    )
    padded = padded_2(paired, (("sp", 1),), 4)
    row_start = lax.axis_index("sp") * rows_dev
    output = attend(query, padded[0], padded[1], table, row_start, rows_dev * lax.axis_size("sp"))
    return (widened + output.reshape(tokens_dev, local_width)).astype(jnp.bfloat16)


def body(
    stream,
    gain_first,
    query_first,
    key_first,
    value_first,
    offset_first,
    gain_second,
    query_second,
    key_second,
    value_second,
    offset_second,
):
    fetched = sent_together(
        (query_first, key_first, value_first, query_second, key_second, value_second), "sp", 0, 1
    )
    first_set = fetched[:3]
    second_set = fetched[3:]
    middle = layer(stream, gain_first, offset_first, first_set)
    return layer(middle, gain_second, offset_second, second_set)


def solution(mesh):
    placed = (
        P("sp", "tp"),
        P("tp"),
        P("sp", "tp"),
        P("sp", "tp"),
        P("sp", "tp"),
        P("tp", None, None),
        P("tp"),
        P("sp", "tp"),
        P("sp", "tp"),
        P("sp", "tp"),
        P("tp", None, None),
    )
    return jax.shard_map(body, mesh=mesh, in_specs=placed, out_specs=P("sp", "tp"), check_vma=False)
```

profile of v0, /device:TPU:1, one launch (start us, length us, event | category | flops | bytes accessed | tf_op | source)
XLA Modules:
  0.0 337.3 jit_solution(11450175371349849308)
XLA Ops:
  6.5 1.6 pad_maximum_fusion.2
  8.2 0.9 constant_dynamic-update-slice_fusion.5
  9.1 0.9 constant_dynamic-update-slice_fusion.4
  9.9 0.9 constant_dynamic-update-slice_fusion.3
  10.8 0.9 constant_dynamic-update-slice_fusion.2
  11.7 0.9 constant_dynamic-update-slice_fusion.1
  12.5 0.9 constant_dynamic-update-slice_fusion
  14.4 0.8 copy.40
  15.9 5.5 %gather_fusion.5 = f32[2048,15]{1,0:T(8,128)S(1)} fusion(f32[15,31]{0,1:T(8,128)S(1)} %bitcast.128, s32[2048]{0:T(1024)S(1)} %broadcast_clamp_fusion), kind=kCustom, calls=%fused_computation.7 | custom fusion | bytes 253952 | tf_op jit(solution)/shard_map/gather | solution.py:56
  22.0 2.0 gather_fusion.12
  24.1 72.0 %all-gather.4.cloned.1.call-done = bf16[4096,513]{0,1:T(8,128)(2,1)} async-done(((bf16[128,513]{0,1:T(8,128)(2,1)}), bf16[4096,513]{0,1:T(8,128)(2,1)}) %all-gather.4.cloned.1.call-update) | async-done | bytes 4202512 | tf_op jit(solution)/shard_map/all_gather | solution.py:16
  96.1 3.1 fusion
  99.2 0.9 slice_convert_fusion.1
  100.0 5.9 %fusion.2 = bf16[4096,512]{0,1:T(8,128)(2,1)} fusion(f32[4096]{0:T(1024)S(1)} %bitcast.154, f32[512]{0:T(512)S(1)} %add_rsqrt_fusion.1, bf16[4096,513]{0,1:T(8,128)(2,1)} %all-gather.4.cloned.1.call-done), kind=kLoop, calls=%fused_computation.20 | loop fusion | flops 8388608 | bytes 8407040 | tf_op jit(solution)/shard_map/convert_element_type | solution.py:94
  105.9 64.6 %all-gather.6.cloned.1.call-done = bf16[4096,768]{1,0:T(8,128)(2,1)} async-done(((bf16[256,768]{1,0:T(8,128)(2,1)}), bf16[4096,768]{1,0:T(8,128)(2,1)}) %all-gather.6.cloned.1.call-update) | async-done | bytes 6291472 | tf_op jit(solution)/shard_map/all_gather | solution.py:43
  170.5 3.9 %convolution_convert_fusion.5 = bf16[512,128]{1,0:T(8,128)(2,1)S(1)} fusion(bf16[4096,512]{0,1:T(8,128)(2,1)} %fusion.2, bf16[4096,768]{1,0:T(8,128)(2,1)} %all-gather.6.cloned.1.call-done), kind=kOutput, calls=%fused_computation.53 | convolution fusion | flops 536936448 | bytes 5373952 | tf_op jit(solution)/shard_map/dot_general | solution.py:98
  174.4 2.5 convolution_convert_fusion.4
  176.9 3.1 collective-permute-start
  180.1 1.5 collective-permute-start.1
  181.5 2.5 convolution_convert_fusion.3
  184.6 1.1 collective-permute-done.1
  185.9 0.8 gather_fusion.3
  188.8 2.6 gather_fusion.4
  191.4 2.6 gather_fusion.1
  194.0 5.2 %fusion.41 = (f32[8,4,16]{2,1,0:T(4,128)S(1)}, f32[8,1,4,16,8,32]{5,3,4,2,0,1:T(8,128)S(1)}) fusion(f32[8,1,8,4,16,32]{5,4,3,2,0,1:T(8,128)} %bitcast.132, pred[8,8]{1,0:T(8,128)(4,1)S(1)} %compare_and_fusion, bf16[8,4,16,128,1]{3,2,4,1,0:T(8,128)(2,1)S(1)} %bitcast.142, bf16[4,32,8,8,128]{4,3,2,1,0:T(8,128)(2,1)} %bitcast.135, ...), kind=kOutput, calls=%fused_computation.105 | convolution fusion | flops 34209280 | bytes 3280960 | tf_op jit(solution)/shard_map/vmap(jqhe,mjkhe->hjqmk)/dot_general | solution.py:70
  199.7 1.1 copy-done.2
  200.7 2.0 fusion.14
  203.6 5.6 %gather_fusion.11 = f32[2048,15]{1,0:T(8,128)S(1)} fusion(f32[15,31]{0,1:T(8,128)S(1)} %bitcast.129, s32[2048]{0:T(1024)S(1)} %broadcast_clamp_fusion), kind=kCustom, calls=%fused_computation.13 | custom fusion | bytes 253952 | tf_op jit(solution)/shard_map/gather | solution.py:56
  210.5 78.9 %all-gather.8.cloned.1.call-done = bf16[4096,513]{0,1:T(8,128)(2,1)} async-done(((bf16[128,513]{0,1:T(8,128)(2,1)}), bf16[4096,513]{0,1:T(8,128)(2,1)}) %all-gather.8.cloned.1.call-update) | async-done | bytes 4202512 | tf_op jit(solution)/shard_map/all_gather | solution.py:16
  289.4 3.2 fusion.3
  292.6 0.9 slice_convert_fusion
  293.5 4.0 %fusion.5 = bf16[4096,512]{0,1:T(8,128)(2,1)S(1)} fusion(f32[4096]{0:T(1024)S(1)} %bitcast.155, f32[512]{0:T(512)S(1)} %add_rsqrt_fusion, bf16[4096,513]{0,1:T(8,128)(2,1)} %all-gather.8.cloned.1.call-done), kind=kLoop, calls=%fused_computation.23 | loop fusion | flops 8388608 | bytes 8407040 | tf_op jit(solution)/shard_map/convert_element_type | solution.py:94
  297.5 1.2 convolution_convert_fusion.1
  298.8 1.2 convolution_convert_fusion.2
  300.1 3.1 collective-permute-start.2
  303.2 1.6 collective-permute-start.3
  304.7 1.2 convolution_convert_fusion
  306.0 1.2 gather_fusion.8
  307.2 2.3 collective-permute-done.3
  309.7 1.7 gather_fusion.9
  311.3 1.9 copy.47
  313.2 2.5 gather_fusion.10
  315.8 1.6 gather_fusion.6
  317.4 1.9 copy.43
  319.4 2.5 gather_fusion.7
  321.9 4.5 %fusion.42 = (f32[8,4,16]{2,1,0:T(4,128)S(1)}, f32[8,1,4,16,8,32]{5,3,4,2,0,1:T(8,128)S(1)}) fusion(f32[8,1,8,4,16,32]{5,4,3,2,0,1:T(8,128)S(1)} %bitcast.133, pred[8,8]{1,0:T(8,128)(4,1)S(1)} %copy-done.9, bf16[8,4,16,128,1]{3,2,4,1,0:T(8,128)(2,1)S(1)} %bitcast.141, bf16[4,32,8,8,128]{4,3,2,1,0:T(8,128)(2,1)} %bitcast.134, ...), kind=kOutput, calls=%fused_computation.106 | convolution fusion | flops 34209280 | bytes 3280960 | tf_op jit(solution)/shard_map/vmap(jqhe,mjkhe->hjqmk)/dot_general | solution.py:70
  327.0 1.1 copy-done.1
  328.1 2.0 fusion.9
  (67 shorter events, 9.4 us)
Async XLA Ops:
  6.5 89.5 %all-gather.4.cloned.1.call-start = ((), (), s32[]{:S(2)}) async-start(), calls=%async_computation | async-start | bytes 4392960 | tf_op jit(solution)/shard_map/all_gather | solution.py:16
  8.2 162.4 %all-gather.6.cloned.1.call-start = ((), (), s32[]{:S(2)}) async-start(), calls=%async_computation.1 | async-start | bytes 6684672 | tf_op jit(solution)/shard_map/all_gather | solution.py:43
  13.4 0.7 copy-start.3
  14.2 275.2 %all-gather.8.cloned.1.call-start = ((), (), s32[]{:S(2)}) async-start(), calls=%async_computation.2 | async-start | bytes 4392960 | tf_op jit(solution)/shard_map/all_gather | solution.py:16
  22.0 2.0 copy-start.12
  24.1 169.9 %copy-start.8 = (pred[8,8]{1,0:T(8,128)(4,1)}, pred[8,8]{1,0:T(8,128)(4,1)S(1)}, u32[]{:S(2)}) copy-start(pred[8,8]{1,0:T(8,128)(4,1)S(1)} %compare_and_fusion) | copy-start | bytes 196
  170.5 3.9 %copy-start = (bf16[4096,512]{0,1:T(8,128)(2,1)S(1)}, bf16[4096,512]{0,1:T(8,128)(2,1)}, u32[]{:S(2)}) copy-start(bf16[4096,512]{0,1:T(8,128)(2,1)} %fusion.2) | copy-start | bytes 12582916
  176.9 7.7 %collective-permute-start = (bf16[2,4,64,1,128]{4,2,1,3,0:T(8,128)(2,1)S(1)}, bf16[2,4,64,1,128]{4,2,1,3,0:T(8,128)(2,1)S(1)}, u32[]{:S(2)}, u32[]{:S(2)}) collective-permute-start(bf16[2,4,64,1,128]{4,2,1,3,0:T(8,128)(2,1)S(1)} %get-tuple-element.12), channel_id=1, source_target_pairs={{0,32},{32,64},{64,96},{96,128},{128,160},{160,192},{192,224},{224... | collective-permute-start | bytes 393224 | tf_op jit(solution)/shard_map/ppermute | solution.py:29
  180.1 5.7 %collective-permute-start.1 = (bf16[2,4,64,1,128]{4,2,1,3,0:T(8,128)(2,1)S(1)}, bf16[2,4,64,1,128]{4,2,1,3,0:T(8,128)(2,1)S(1)}, u32[]{:S(2)}, u32[]{:S(2)}) collective-permute-start(bf16[2,4,64,1,128]{4,2,1,3,0:T(8,128)(2,1)S(1)} %get-tuple-element.13), channel_id=1, source_target_pairs={{32,0},{64,32},{96,64},{128,96},{160,128},{192,160},{224,192},{256... | collective-permute-start | bytes 393224 | tf_op jit(solution)/shard_map/ppermute | solution.py:32
  191.4 2.6 copy-start.6
  199.1 1.6 copy-start.2
  200.7 2.0 copy-start.5
  200.7 2.0 copy-start.11
  200.7 2.7 copy-start.10
  289.4 8.1 %slice-start = ((s8[6291456]{0:T(1024)(128)(4,1)}), s8[4194304]{0:T(1024)(128)(4,1)S(1)}, s32[]{:S(2)}) async-start(s8[6291456]{0:T(1024)(128)(4,1)} %bitcast.158), calls=%async_computation.3 | async-start | bytes 8388608
  293.5 4.0 %slice-start.1 = ((s8[6291456]{0:T(1024)(128)(4,1)}), s8[2097152]{0:T(1024)(128)(4,1)S(1)}, s32[]{:S(2)}) async-start(s8[6291456]{0:T(1024)(128)(4,1)} %bitcast.158), calls=%async_computation.4 | async-start | bytes 4194304
  300.1 7.2 %collective-permute-start.2 = (bf16[2,4,64,1,128]{4,2,1,3,0:T(8,128)(2,1)S(1)}, bf16[2,4,64,1,128]{4,2,1,3,0:T(8,128)(2,1)S(1)}, u32[]{:S(2)}, u32[]{:S(2)}) collective-permute-start(bf16[2,4,64,1,128]{4,2,1,3,0:T(8,128)(2,1)S(1)} %get-tuple-element.10), channel_id=1, source_target_pairs={{0,32},{32,64},{64,96},{96,128},{128,160},{160,192},{192,224},{224... | collective-permute-start | bytes 393224 | tf_op jit(solution)/shard_map/ppermute | solution.py:29
  303.2 6.4 %collective-permute-start.3 = (bf16[2,4,64,1,128]{4,2,1,3,0:T(8,128)(2,1)S(1)}, bf16[2,4,64,1,128]{4,2,1,3,0:T(8,128)(2,1)S(1)}, u32[]{:S(2)}, u32[]{:S(2)}) collective-permute-start(bf16[2,4,64,1,128]{4,2,1,3,0:T(8,128)(2,1)S(1)} %get-tuple-element.11), channel_id=1, source_target_pairs={{32,0},{64,32},{96,64},{128,96},{160,128},{192,160},{224,192},{256... | collective-permute-start | bytes 393224 | tf_op jit(solution)/shard_map/ppermute | solution.py:32
  319.4 2.6 copy-start.4
  319.4 2.5 copy-start.7
  319.4 2.5 copy-start.9
  326.5 1.6 copy-start.1
Sparse Core Ops, SparseCore 0:
  9.4 86.6 all-gather.3
  99.1 71.4 all-gather.5
  203.6 85.7 all-gather.7
where the time goes:
time: 340 us; the launch traced here: 337 us
  waiting for transfers between devices  219 us (64%)
  local copies, waits for them, and re-layouts  46.2 us (14%)
  matrix products  26.2 us (8%)
  other arithmetic  23.1 us (7%)
  between operations  13.5 us (4%)
  starting transfers between devices  9.31 us (3%)
    all_gather x2, waiting for transfers between devices, turned_gather(): lax.all_gather(both, axis, axis=0, tiled=True)  151 us
    all_gather x1, waiting for transfers between devices, sent_together(): lax.all_gather(both, axis, axis=dim, tiled=True)  64.6 us
    gather x4, local copies, waits for them, and re-layouts, attend(): column_bias = table[:, :, column_offset]  12.3 us
    gather x6, local copies, waits for them, and re-layouts, one_row(): key_block = lax.dynamic_slice_in_dim(keys, local, 8, 0)[:, key_cols]  10.2 us
    gather x6, local copies, waits for them, and re-layouts, one_row(): value_block = lax.dynamic_slice_in_dim(values, local, 8, 0)[:, key_cols]  10.1 us
    convert_element_type x2, other arithmetic, layer(): (full_wide * lax.rsqrt(mean_square + epsilon) * full_gain.astype(jnp.floa...  9.88 us
    dot_general x2, matrix products, one_row(): jnp.einsum('jqhe,mjkhe->hjqmk', query_row, key_block, preferred_element_t...  9.71 us
    unnamed x37, local copies, waits for them, and re-layouts  8.13 us
  transfers between devices with their start and end apart: 7, of which 5 were waited for; matrix products, arithmetic and copies ran while one was open for 11% of the time, Pallas kernels for 0%

commit v1 on v0

v1 whole, which is shorter than its diff:
```python
import functools

import jax
import jax.numpy as jnp
from jax import lax
from jax.experimental import pallas as pl
from jax.experimental.pallas import tpu as pltpu
from jax.sharding import PartitionSpec as P

GRID_W = 64
HEAD = 128
ROWS = 8
TOK = ROWS * GRID_W
HALF = TOK // 2
PAD = 16
SIDE = 4
EPS = 1e-6
BLOCK = 2 * HEAD
LOW = 4 * GRID_W
HIGH = 3 * GRID_W
X, Y = 0, 1
LINKS = ((X, 1), (X, -1), (Y, 1), (Y, -1))
MESH_ID = pl.DeviceIdType.MESH


def weight_messages(axis, sign):
    part = 0 if sign > 0 else 1
    half = 1 if axis == X else 0
    own_first = 0 if axis == X else 2
    return (
        ("0a", (0, 0), own_first, 2),
        ("0b", (0, 0), 2 - own_first, 2),
        ("1a", (0, -1), 2 * half, 2),
        ("1a", (0, 1), 2 * half, 2),
        ("1a", (-sign, 0), own_first + part, 1),
        ("1b", (-sign, 0), 2 - own_first + part, 1),
        ("2a", (0, 2), 2 * half, 2),
        ("2b", (-sign, -1), 2 * half + part, 1),
        ("2b", (-sign, 1), 2 * half + part, 1),
        ("3", (-sign, 2), 2 * half + part, 1),
    )


SEND_AT = {
    (0, 0): (("send", 0, "0a"), ("send", 0, "0b")),
    (0, 1): (("wait", 0, "0a"), ("send", 0, "1a")),
    (0, 2): (("wait", 0, "0b"), ("send", 0, "1b")),
    (0, 4): (("wait", 0, "1a"), ("send", 0, "2a"), ("send", 0, "2b")),
    (0, 6): (("wait", 0, "2a"), ("send", 0, "3"), ("send", 1, "0a"), ("send", 1, "0b")),
    (0, 7): (("wait", 0, "1b"), ("wait", 0, "2b"), ("wait", 0, "3")),
    (1, 0): (("wait", 1, "0a"), ("wait", 1, "0b"), ("send", 1, "1a"), ("send", 1, "1b")),
    (1, 3): (("wait", 1, "1a"), ("wait", 1, "1b"), ("send", 1, "2a"), ("send", 1, "2b")),
    (1, 5): (("wait", 1, "2a"), ("send", 1, "3")),
    (1, 6): (("wait", 1, "2b"), ("wait", 1, "3")),
}


def kernel(
    zn,
    x_hbm,
    gains_hbm,
    q0_hbm,
    k0_hbm,
    v0_hbm,
    q1_hbm,
    k1_hbm,
    v1_hbm,
    table0,
    table1,
    out,
    xg,
    weights,
    kv,
    query,
    acc,
    square,
    tab,
    bias,
    local_sem,
    z_send,
    z_recv,
    core_send,
    core_recv,
    w_send,
    w_recv,
    halo_send,
    halo_recv,
):
    sp = lax.axis_index("sp")
    tp = lax.axis_index("tp")
    n_sp = SIDE * SIDE
    gx, gy = lax.rem(sp, SIDE), lax.div(sp, SIDE)
    core, z = lax.rem(tp, 2), lax.div(tp, 2)
    steps = zn // 2
    shards = n_sp // zn
    features = zn * BLOCK

    def at_z(offset):
        return lax.rem(z + offset + zn, zn)

    def chip(z_at, core_at):
        return {"sp": sp, "tp": z_at * 2 + core_at}

    def grid_sp(dx, dy):
        return lax.rem(gy + dy + SIDE, SIDE) * SIDE + lax.rem(gx + dx + SIDE, SIDE)

    def around(axis, along, across):
        along, across = (along + SIDE) % SIDE, (across + SIDE) % SIDE
        return grid_sp(along, across) if axis == X else grid_sp(across, along)

    sibling = chip(z, 1 - core)
    z_next, z_prev = chip(at_z(1), core), chip(at_z(-1), core)
    sp_next = {"sp": lax.rem(sp + 1, n_sp), "tp": tp}
    sp_prev = {"sp": lax.rem(sp + n_sp - 1, n_sp), "tp": tp}

    own = xg.at[0, z, core]
    loads = [
        pltpu.make_async_copy(x_hbm, own.at[0:TOK], local_sem.at[0]),
        pltpu.make_async_copy(gains_hbm, own.at[TOK : TOK + PAD], local_sem.at[1]),
    ]
    for layer, refs in enumerate(((q0_hbm, k0_hbm, v0_hbm), (q1_hbm, k1_hbm, v1_hbm))):
        for m, ref in enumerate(refs):
            loads.append(
                pltpu.make_async_copy(
                    ref, weights.at[layer, sp, :, m], local_sem.at[2 + 3 * layer + m]
                )
            )
    for load in loads:
        load.start()

    barrier = pltpu.get_barrier_semaphore()
    peers = [z_next, z_prev, sibling, sp_next, sp_prev]
    peers += [{"sp": around(axis, sign, 0), "tp": tp} for axis, sign in LINKS]
    for peer in peers:
        pl.semaphore_signal(barrier, inc=1, device_id=peer, device_id_type=MESH_ID)

    lanes = lax.broadcasted_iota(jnp.int32, (GRID_W, HEAD), 1) & (GRID_W - 1)
    column = lax.broadcasted_iota(jnp.int32, (GRID_W, HEAD), 0)
    first_column = jnp.clip(column - 8, 0, GRID_W - 16)
    in_window = (lanes >= first_column) & (lanes < first_column + 16)
    for layer, table in enumerate((table0, table1)):
        tab[...] = jnp.zeros_like(tab)
        tab[0:15, 0:31] = table[0]
        rows = tab[...]
        both = rows + pltpu.roll(pltpu.roll(rows, 15, 0), GRID_W, 1)
        for offset in range(14):
            spread = jnp.broadcast_to(both[offset : offset + 1], (GRID_W, HEAD))
            band = pltpu.roll(spread, HEAD - 15, 1, stride=1, stride_axis=0)
            bias[layer, offset] = jnp.where(in_window, band, -1e30)

    pl.semaphore_wait(barrier, len(peers))

    def remote(src, dst, send_sem, recv_sem, device):
        return pltpu.make_async_remote_copy(
            src_ref=src,
            dst_ref=dst,
            send_sem=send_sem,
            recv_sem=recv_sem,
            device_id=device,
            device_id_type=MESH_ID,
        )

    def chunk_rows(layer, chunk):
        if chunk == 0:
            return pl.ds(0, HALF)
        return pl.ds(HALF, HALF + (PAD if layer == 0 else 0))

    def z_copy(layer, origin, chunk, direction, step):
        ref = xg.at[layer, origin, core, chunk_rows(layer, chunk)]
        return remote(
            ref,
            ref,
            z_send.at[layer],
            z_recv.at[layer, direction, step, chunk],
            z_next if direction == 0 else z_prev,
        )

    def core_copy(layer, origin, chunk, from_core):
        ref = xg.at[layer, origin, from_core, chunk_rows(layer, chunk)]
        return remote(ref, ref, core_send.at[layer], core_recv.at[layer, origin, chunk], sibling)

    def weight_copy(layer, link, index, inbound):
        axis, sign = LINKS[link]
        _, (along, across), piece, pieces = weight_messages(axis, sign)[index]
        origin = around(axis, along - (sign if inbound else 0), across)
        ref = weights.at[layer, origin, pl.ds(piece, pieces)]
        return remote(
            ref,
            ref,
            w_send.at[layer],
            w_recv.at[layer, link, index],
            {"sp": around(axis, sign, 0), "tp": tp},
        )

    def weight_round(action, layer, name):
        for index in range(10):
            for link, (axis, sign) in enumerate(LINKS):
                if weight_messages(axis, sign)[index][0] == name:
                    copy = weight_copy(layer, link, index, action == "wait")
                    if action == "wait":
                        copy.wait_recv()
                    else:
                        copy.start()

    def add_block(layer, origin):
        for chunk in range(2):
            core_copy(layer, origin, chunk, 1 - core).wait_recv()
        columns = []
        for m in range(3):
            pieces = weights[layer, pl.ds(origin * shards, shards), :, m]
            columns.append(pieces.reshape(BLOCK, HEAD))
        right = jnp.concatenate(columns, axis=1)
        gains = [
            xg[0, origin, c, TOK : TOK + PAD, :].astype(jnp.float32)[layer : layer + 1]
            for c in range(2)
        ]
        for top in range(0, TOK, 128):
            rows = slice(top, top + 128)
            scaled, squares = [], square[rows, :]
            for c in range(2):
                wide = xg[layer, origin, c, rows, :].astype(jnp.float32)
                squares = squares + wide * wide
                scaled.append((wide * gains[c]).astype(jnp.bfloat16))
            square[rows, :] = squares
            acc[rows, :] += jnp.dot(
                jnp.concatenate(scaled, axis=1), right, preferred_element_type=jnp.float32
            )

    def blocks_between(layer, low, high):
        @pl.loop(low, high)
        def _(offset):
            add_block(layer, at_z(offset))

    def gather_step(layer, step):
        last = step == steps
        for chunk in range(2):
            for direction in range(2):
                if last and chunk != direction:
                    continue
                origin = at_z(-step if direction == 0 else step)
                if step > 0:
                    z_copy(layer, origin, chunk, direction, step - 1).wait_recv()
                if step < steps - 1 or (step == steps - 1 and chunk == direction):
                    z_copy(layer, origin, chunk, direction, step).start()
                if step > 0 or direction == 0:
                    core_copy(layer, origin, chunk, core).start()

    def project(layer):
        mean = jnp.sum(square[...], axis=1, keepdims=True) * (1.0 / features)
        scale = lax.rsqrt(mean + EPS)
        kv[layer, LOW : LOW + TOK, :] = (acc[:, HEAD:] * scale).astype(jnp.bfloat16)
        query[...] = (acc[:, :HEAD] * scale).astype(jnp.bfloat16)

    def halo_copies(layer):
        up = remote(
            kv.at[layer, pl.ds(TOK, LOW)],
            kv.at[layer, pl.ds(0, LOW)],
            halo_send.at[layer, 0],
            halo_recv.at[layer, 0],
            sp_next,
        )
        down = remote(
            kv.at[layer, pl.ds(LOW, HIGH)],
            kv.at[layer, pl.ds(LOW + TOK, HIGH)],
            halo_send.at[layer, 1],
            halo_recv.at[layer, 1],
            sp_prev,
        )
        return up, down

    def attend(layer, row):
        grid_row = sp * ROWS + row
        first = jnp.clip(grid_row - 4, 0, n_sp * ROWS - 8)
        start = pl.multiple_of((first - sp * ROWS + 4) * GRID_W, GRID_W)
        offset = first - grid_row + 7
        window = pl.ds(start, 8 * GRID_W)
        score = lax.dot_general(
            query[row * GRID_W : (row + 1) * GRID_W, :],
            kv[layer, window, 0:HEAD],
            (((1,), (1,)), ((), ())),
            preferred_element_type=jnp.float32,
        )
        bands = jnp.concatenate([bias[layer, offset + 2 * m] for m in range(4)], axis=1)
        score = score * (HEAD**-0.5) + bands
        weight = jnp.exp(score - jnp.max(score, axis=1, keepdims=True))
        total = jnp.sum(weight, axis=1, keepdims=True)
        mixed = jnp.dot(
            weight.astype(jnp.bfloat16), kv[layer, window, HEAD:], preferred_element_type=jnp.float32
        )
        return mixed / total

    loads[0].wait()
    loads[1].wait()
    for layer in range(2):
        acc[...] = jnp.zeros_like(acc)
        square[...] = jnp.zeros_like(square)
        for step in range(steps + 1):
            if layer == 0 or step > 0:
                gather_step(layer, step)
            if layer == 0 and step == 0:
                for load in loads[2:]:
                    load.wait()
            for at in range(8):
                if at == step or (step == steps and at > step):
                    for action, which, name in SEND_AT.get((layer, at), ()):
                        weight_round(action, which, name)
            if step == max(steps - 1, 1):
                blocks_between(layer, 1 - steps, steps)
        add_block(layer, at_z(steps))
        project(layer)
        up, down = halo_copies(layer)
        up.start()
        down.start()
        up.wait_recv()
        down.wait_recv()
        for chunk in range(2):
            for row in range(4 * chunk, 4 * chunk + 4):
                rows = slice(row * GRID_W, (row + 1) * GRID_W)
                x = xg[layer, z, core, rows, :].astype(jnp.float32)
                result = (x + attend(layer, row)).astype(jnp.bfloat16)
                if layer == 0:
                    xg[1, z, core, rows, :] = result
                else:
                    out[rows, :] = result
            if layer == 0:
                for direction in range(2):
                    if steps > 1 or chunk == direction:
                        z_copy(1, z, chunk, direction, 0).start()
                core_copy(1, z, chunk, core).start()

    for layer in range(2):
        rows = pl.ds(0, TOK + (PAD if layer == 0 else 0))
        sent = xg.at[layer, pl.ds(0, zn - 1), 0, rows]
        remote(sent, sent, z_send.at[layer], z_recv.at[layer, 0, 0, 0], z_next).wait_send()
        sent = xg.at[layer, pl.ds(0, zn), 0, rows]
        remote(sent, sent, core_send.at[layer], core_recv.at[layer, 0, 0], sibling).wait_send()
        sent = weights.at[layer, pl.ds(0, n_sp - 1)]
        remote(sent, sent, w_send.at[layer], w_recv.at[layer, 0, 0], sp_next).wait_send()
        for copy in halo_copies(layer):
            copy.wait_send()


def body(zn, x, gain0, q0, k0, v0, table0, gain1, q1, k1, v1, table1):
    gains = jnp.pad(jnp.stack([gain0, gain1]), ((0, PAD - 2), (0, 0)))
    piece = q0.shape[0] // 4
    pieces = [w.reshape(4, piece, HEAD) for w in (q0, k0, v0, q1, k1, v1)]
    steps = zn // 2
    n_sp = SIDE * SIDE
    hbm = pl.BlockSpec(memory_space=pltpu.HBM)
    vmem = pl.BlockSpec(memory_space=pltpu.VMEM)
    dma = pltpu.SemaphoreType.DMA
    return pl.pallas_call(
        functools.partial(kernel, zn),
        out_shape=jax.ShapeDtypeStruct((TOK, HEAD), jnp.bfloat16),
        in_specs=[hbm] * 8 + [vmem] * 2,
        out_specs=vmem,
        scratch_shapes=[
            pltpu.VMEM((2, zn, 2, TOK + PAD, HEAD), jnp.bfloat16),
            pltpu.VMEM((2, n_sp, 4, 3, piece, HEAD), jnp.bfloat16),
            pltpu.VMEM((2, LOW + TOK + 4 * GRID_W, 2 * HEAD), jnp.bfloat16),
            pltpu.VMEM((TOK, HEAD), jnp.bfloat16),
            pltpu.VMEM((TOK, 3 * HEAD), jnp.float32),
            pltpu.VMEM((TOK, HEAD), jnp.float32),
            pltpu.VMEM((16, HEAD), jnp.float32),
            pltpu.VMEM((2, 14, GRID_W, HEAD), jnp.float32),
            dma((8,)),
            dma((2,)),
            dma((2, 2, steps, 2)),
            dma((2,)),
            dma((2, zn, 2)),
            dma((2,)),
            dma((2, 4, 10)),
            dma((2, 2)),
            dma((2, 2)),
        ],
        compiler_params=pltpu.CompilerParams(
            collective_id=0, has_side_effects=True, vmem_limit_bytes=48 * 1024 * 1024
        ),
        name="neighbourhood",
    )(x, gains, *pieces, table0, table1)


def solution(mesh):
    placed = (
        P("sp", "tp"),
        P("tp"),
        P("sp", "tp"),
        P("sp", "tp"),
        P("sp", "tp"),
        P("tp", None, None),
        P("tp"),
        P("sp", "tp"),
        P("sp", "tp"),
        P("sp", "tp"),
        P("tp", None, None),
    )
    return jax.shard_map(
        functools.partial(body, mesh.shape["tp"] // 2),
        mesh=mesh,
        in_specs=placed,
        out_specs=P("sp", "tp"),
        check_vma=False,
    )
```

time: 340 us -> 109 us (0.32)
  waiting for transfers between devices: 219 us -> 0 us
  Pallas kernels: 0 us -> 101 us
  local copies, waits for them, and re-layouts: 46.2 us -> 7.96 us
  matrix products: 26.2 us -> 0 us
  other arithmetic: 23.1 us -> 0.01 us
  between operations: 13.5 us -> 0.05 us
  starting transfers between devices: 9.31 us -> 0 us
    all_gather x3 -> x0, waiting for transfers between devices: 215 us -> none  [the longest x2 151 us: turned_gather(): lax.all_gather(both, axis, axis=0, tiled=True)]
    pallas_call x0 -> x1, Pallas kernels: none -> 101 us  [body(): pl.pallas_call(functools.partial(kernel, zn), out_shape=jax.ShapeDtypeStr...]
    gather x20 -> x0, local copies, waits for them, and re-layouts: 37 us -> none  [the longest x4 12.3 us: attend(): column_bias = table[:, :, column_offset]]
    dot_general x10 -> x0, matrix products: 26.2 us -> none  [the longest x2 9.71 us: one_row(): jnp.einsum('jqhe,mjkhe->hjqmk', query_row, key_block, preferred_element_t...]
    convert_element_type x6 -> x0, other arithmetic: 12.3 us -> none  [the longest x2 9.88 us: layer(): (full_wide * lax.rsqrt(mean_square + epsilon) * full_gain.astype(jnp.floa...]
    ppermute x4 -> x0, starting transfers between devices: 9.23 us -> none  [the longest x2 6.2 us: padded_2(): lax.ppermute(lax.slice_in_dim(block, block.shape[dim] - width, None, axis...]
    reduce_sum x4 -> x0, other arithmetic: 7.35 us -> none  [the longest x2 6.31 us: layer(): mean_square = jnp.mean(full_wide * full_wide, axis=-1, keepdims=True)]
    ppermute x4 -> x0, waiting for transfers between devices: 3.49 us -> none  [the longest x2 3.48 us: padded_2(): lax.ppermute(lax.slice_in_dim(block, 0, width, axis=dim), axis, backward)]
  transfers between devices with their start and end apart: 7 -> 0, of which waited for: 5 -> 0; matrix products, arithmetic and copies ran while one was open for 11% -> 0% of each run, Pallas kernels for 0% -> 0%
where the time goes in v1:
time: 109 us
  Pallas kernels  101 us (93%)
  local copies, waits for them, and re-layouts  7.96 us (7%)
    pallas_call x1, Pallas kernels, body(): pl.pallas_call(functools.partial(kernel, zn), out_shape=jax.ShapeDtypeStr...  101 us
    unnamed x25, local copies, waits for them, and re-layouts  7.96 us

profile of v1, /device:TPU:1, one launch (start us, length us, event | category | flops | bytes accessed | tf_op | source)
XLA Modules:
  0.0 108.7 jit_solution(17507767797272096609)
XLA Ops:
  0.0 0.0 copy-start.7
  0.0 0.0 copy-start.9
  0.0 0.0 copy-start.10
  0.0 0.7 copy-done.9
  0.7 0.0 copy-done.10
  0.7 0.0 copy-done.7
  0.7 0.0 copy-start.8
  0.7 0.7 copy-done.8
  1.4 0.0 copy-start
  1.4 0.9 copy-done
  2.3 0.0 copy-start.1
  2.3 0.8 copy-done.1
  3.2 0.0 copy-start.2
  3.2 0.8 copy-done.2
  4.0 0.0 copy-start.3
  4.0 0.8 copy-done.3
  4.8 0.0 copy-start.4
  4.8 0.8 copy-done.4
  5.7 0.0 copy-start.5
  5.7 0.8 copy-done.5
  6.5 0.0 copy-start.6
  6.5 0.8 copy-done.6
  7.4 100.7 %neighbourhood.1 = bf16[512,128]{1,0:T(8,128)(2,1)S(1)} custom-call(bf16[512,128]{1,0:T(8,128)(2,1)S(1)} %copy-done, bf16[16,128]{1,0:T(8,128)(2,1)S(1)} %fusion.2.gains_hbm, bf16[4,64,128]{2,1,0:T(8,128)(2,1)S(1)} %bitcast.8, bf16[4,64,128]{2,1,0:T(8,128)(2,1)S(1)} %bitcast.9, bf16[4,64,128]{2,1,0:T(8,128)(2,1)S(1)} %bitcast.10, ...), custom_call_target="tpu_custom_call" | custom-call | tf_op jit(solution)/shard_map/neighbourhood/pallas_call | solution.py:352
  108.1 0.7 copy.15
  (3 shorter events, 0.0 us)
Async XLA Ops:
  0.0 0.7 copy-start.7
  0.0 0.7 copy-start.9
  0.0 0.7 copy-start.10
  0.7 0.7 copy-start.8
  1.4 0.9 copy-start
  2.3 0.8 copy-start.1
  3.2 0.8 copy-start.2
  4.0 0.8 copy-start.3
  4.8 0.8 copy-start.4
  5.7 0.8 copy-start.5
  6.5 0.8 copy-start.6

commit v2 on v1

v2 whole, which is shorter than its diff:
```python
import functools

import jax
import jax.numpy as jnp
from jax import lax
from jax.experimental import pallas as pl
from jax.experimental.pallas import tpu as pltpu
from jax.sharding import PartitionSpec as P

GRID_W = 64
HEAD = 128
ROWS = 8
TOK = ROWS * GRID_W
CHUNKS = 4
PART = TOK // CHUNKS
PAD = 16
SIDE = 4
EPS = 1e-6
BLOCK = 2 * HEAD
LOW = 4 * GRID_W
HIGH = 3 * GRID_W
X, Y = 0, 1
LINKS = ((X, 1), (X, -1), (Y, 1), (Y, -1))
MESH_ID = pl.DeviceIdType.MESH


def weight_messages(axis, sign):
    part = 0 if sign > 0 else 1
    half = 1 if axis == X else 0
    own_first = 0 if axis == X else 2
    return (
        ("0a", (0, 0), own_first, 2),
        ("0b", (0, 0), 2 - own_first, 2),
        ("1a", (0, -1), 2 * half, 2),
        ("1a", (0, 1), 2 * half, 2),
        ("1a", (-sign, 0), own_first + part, 1),
        ("1b", (-sign, 0), 2 - own_first + part, 1),
        ("2a", (0, 2), 2 * half, 2),
        ("2b", (-sign, -1), 2 * half + part, 1),
        ("2b", (-sign, 1), 2 * half + part, 1),
        ("3", (-sign, 2), 2 * half + part, 1),
    )


WEIGHTS_AT = {
    (0, 0): (("send", 0, "0a"), ("send", 0, "0b")),
    (0, 1): (("wait", 0, "0a"), ("send", 0, "1a")),
    (0, 2): (("wait", 0, "0b"), ("send", 0, "1b")),
    (0, 3): (("wait", 0, "1a"), ("send", 0, "2a"), ("send", 0, "2b")),
    (0, 5): (("wait", 0, "2a"), ("send", 0, "3"), ("send", 1, "0a"), ("send", 1, "0b")),
    (0, 6): (("wait", 0, "1b"), ("wait", 0, "2b"), ("wait", 0, "3")),
    (0, "halo"): (("wait", 1, "0a"), ("wait", 1, "0b"), ("send", 1, "1a"), ("send", 1, "1b")),
    (1, 2): (("wait", 1, "1a"), ("wait", 1, "1b"), ("send", 1, "2a"), ("send", 1, "2b")),
    (1, 4): (("wait", 1, "2a"), ("send", 1, "3")),
    (1, 5): (("wait", 1, "2b"), ("wait", 1, "3")),
}
BLOCKS_AT = {
    (0, 7): (range(-6, -2), range(-2, 2), range(2, 7)),
    (0, 8): ((-7, 7),),
    (1, 6): (range(-5, -1), range(-1, 2), range(2, 6)),
    (1, 7): ((-6, 6),),
    (1, 8): ((-7, 7),),
}
MASKED = -1e30


def kernel(
    zn,
    x_hbm,
    gain0_hbm,
    gain1_hbm,
    q0_hbm,
    k0_hbm,
    v0_hbm,
    q1_hbm,
    k1_hbm,
    v1_hbm,
    table0_hbm,
    table1_hbm,
    out,
    xg,
    weights,
    kv,
    query,
    acc,
    square,
    own_gains,
    gains,
    tables,
    tab,
    band,
    own_bias,
    low_bias,
    high_bias,
    local_sem,
    z_send,
    z_recv,
    core_send,
    core_recv,
    gain_send,
    gain_recv,
    gain_core_send,
    gain_core_recv,
    w_send,
    w_recv,
    halo_send,
    halo_recv,
):
    sp = lax.axis_index("sp")
    tp = lax.axis_index("tp")
    n_sp = SIDE * SIDE
    gx, gy = lax.rem(sp, SIDE), lax.div(sp, SIDE)
    core, z = lax.rem(tp, 2), lax.div(tp, 2)
    steps = zn // 2
    shards = n_sp // zn
    features = zn * BLOCK

    def at_z(offset):
        return lax.rem(z + offset + zn, zn)

    def chip(z_at, core_at):
        return {"sp": sp, "tp": z_at * 2 + core_at}

    def grid_sp(dx, dy):
        return lax.rem(gy + dy + SIDE, SIDE) * SIDE + lax.rem(gx + dx + SIDE, SIDE)

    def around(axis, along, across):
        along, across = (along + SIDE) % SIDE, (across + SIDE) % SIDE
        return grid_sp(along, across) if axis == X else grid_sp(across, along)

    sibling = chip(z, 1 - core)
    z_next, z_prev = chip(at_z(1), core), chip(at_z(-1), core)
    sp_next = {"sp": lax.rem(sp + 1, n_sp), "tp": tp}
    sp_prev = {"sp": lax.rem(sp + n_sp - 1, n_sp), "tp": tp}

    loads = [
        pltpu.make_async_copy(x_hbm, xg.at[0, z, core], local_sem.at[0]),
        pltpu.make_async_copy(gain0_hbm, own_gains.at[0], local_sem.at[1]),
        pltpu.make_async_copy(gain1_hbm, own_gains.at[1], local_sem.at[2]),
        pltpu.make_async_copy(table0_hbm, tables.at[0], local_sem.at[3]),
        pltpu.make_async_copy(table1_hbm, tables.at[1], local_sem.at[4]),
    ]
    for layer, refs in enumerate(((q0_hbm, k0_hbm, v0_hbm), (q1_hbm, k1_hbm, v1_hbm))):
        for m, ref in enumerate(refs):
            loads.append(
                pltpu.make_async_copy(
                    ref, weights.at[layer, sp, :, m], local_sem.at[5 + 3 * layer + m]
                )
            )
    for load in loads:
        load.start()

    barrier = pltpu.get_barrier_semaphore()
    peers = [z_next, z_prev, sibling, sp_next, sp_prev]
    peers += [{"sp": around(axis, sign, 0), "tp": tp} for axis, sign in LINKS]
    for peer in peers:
        pl.semaphore_signal(barrier, inc=1, device_id=peer, device_id_type=MESH_ID)

    loads[1].wait()
    loads[2].wait()
    spare = jnp.zeros((PAD - 2, HEAD), jnp.float32)
    both_gains = [own_gains[layer].astype(jnp.float32) for layer in range(2)]
    gains[z, core] = jnp.concatenate(both_gains + [spare]).astype(jnp.bfloat16)
    for layer in range(2):
        kv[layer, LOW + TOK + HIGH :, :] = jnp.zeros((GRID_W, 2 * HEAD), jnp.bfloat16)

    def build_bias(layer):
        lanes = lax.broadcasted_iota(jnp.int32, (GRID_W, HEAD), 1)
        key_column = lanes & (GRID_W - 1)
        column = lax.broadcasted_iota(jnp.int32, (GRID_W, HEAD), 0)
        first_column = jnp.clip(column - 8, 0, GRID_W - 16)
        in_window = (key_column >= first_column) & (key_column < first_column + 16)
        tab[...] = jnp.zeros_like(tab)
        tab[0:15, 0:31] = tables[layer, :, 0, :]
        rows = tab[...]
        both = rows + pltpu.roll(pltpu.roll(rows, 15, 0), GRID_W, 1)
        for offset in range(14):
            spread = jnp.broadcast_to(both[offset : offset + 1], (GRID_W, HEAD))
            shifted = pltpu.roll(spread, HEAD - 15, 1, stride=1, stride_axis=0)
            band[offset] = jnp.where(in_window, shifted, MASKED)
        at_start = jnp.where(sp == 0, 0.0, MASKED)
        at_end = jnp.where(sp == n_sp - 1, 0.0, MASKED)
        not_start = jnp.where(sp == 0, MASKED, 0.0)
        not_end = jnp.where(sp == n_sp - 1, MASKED, 0.0)
        right = lanes >= GRID_W

        def pair(row, key_row, penalties):
            if penalties == (None, None):
                return jnp.full((GRID_W, HEAD), MASKED, jnp.float32)
            values = [MASKED if p is None else p for p in penalties]
            offset = key_row - row + 7
            base = band[offset]
            return base + jnp.where(right, values[1], values[0])

        def inside(row, key_row):
            return row - 4 <= key_row <= row + 3

        for row in range(ROWS):
            for m in range(0, ROWS, 2):
                penalties = tuple(
                    0.0 if inside(row, m + d) else (at_start if row < 4 else at_end)
                    for d in range(2)
                )
                own_bias[layer, row, :, m * GRID_W : (m + 2) * GRID_W] = pair(row, m, penalties)
            for m in range(0, 4, 2):
                lanes_at = slice(m * GRID_W, (m + 2) * GRID_W)
                if row < 4:
                    penalties = tuple(
                        not_start if inside(row, m + d - 4) else None for d in range(2)
                    )
                    low_bias[layer, row, :, lanes_at] = pair(row, m - 4, penalties)
                else:
                    penalties = tuple(not_end if inside(row, m + d + 8) else None for d in range(2))
                    high_bias[layer, row - 4, :, lanes_at] = pair(row, m + 8, penalties)

    pl.semaphore_wait(barrier, len(peers))

    def remote(src, dst, send_sem, recv_sem, device):
        return pltpu.make_async_remote_copy(
            src_ref=src,
            dst_ref=dst,
            send_sem=send_sem,
            recv_sem=recv_sem,
            device_id=device,
            device_id_type=MESH_ID,
        )

    def chunk_rows(chunk):
        start = chunk * PART
        return pl.ds(start if isinstance(chunk, int) else pl.multiple_of(start, PART), PART)

    def z_copy(layer, origin, chunk, direction, step):
        ref = xg.at[layer, origin, core, chunk_rows(chunk)]
        return remote(
            ref,
            ref,
            z_send.at[layer],
            z_recv.at[layer, direction, step, chunk],
            z_next if direction == 0 else z_prev,
        )

    def core_copy(layer, origin, chunk, from_core):
        ref = xg.at[layer, origin, from_core, chunk_rows(chunk)]
        return remote(ref, ref, core_send.at[layer], core_recv.at[layer, origin, chunk], sibling)

    def gain_copy(origin, direction, step):
        ref = gains.at[origin, core]
        device = z_next if direction == 0 else z_prev
        return remote(ref, ref, gain_send, gain_recv.at[direction, step], device)

    def gain_core_copy(origin, from_core):
        ref = gains.at[origin, from_core]
        return remote(ref, ref, gain_core_send, gain_core_recv.at[origin], sibling)

    def weight_copy(layer, link, index, inbound):
        axis, sign = LINKS[link]
        _, (along, across), piece, pieces = weight_messages(axis, sign)[index]
        origin = around(axis, along - (sign if inbound else 0), across)
        ref = weights.at[layer, origin, pl.ds(piece, pieces)]
        return remote(
            ref,
            ref,
            w_send.at[layer],
            w_recv.at[layer, link, index],
            {"sp": around(axis, sign, 0), "tp": tp},
        )

    def weight_round(action, layer, name):
        for index in range(10):
            for link, (axis, sign) in enumerate(LINKS):
                if weight_messages(axis, sign)[index][0] == name:
                    copy = weight_copy(layer, link, index, action == "wait")
                    if action == "wait":
                        copy.wait_recv()
                    else:
                        copy.start()

    def add_rows(layer, offsets, chunk):
        rows = chunk_rows(chunk)
        origins = [at_z(offset) for offset in offsets]
        for origin in origins:
            core_copy(layer, origin, chunk, 1 - core).wait_recv()
        squares, scaled, right = square[rows, :], [], []
        for origin in origins:
            for c in range(2):
                wide = xg[layer, origin, c, rows, :].astype(jnp.float32)
                gain = gains[origin, c].astype(jnp.float32)[layer : layer + 1]
                squares = squares + wide * wide
                scaled.append((wide * gain).astype(jnp.bfloat16))
            columns = []
            for m in range(3):
                pieces = weights[layer, pl.ds(origin * shards, shards), :, m]
                columns.append(pieces.reshape(BLOCK, HEAD))
            right.append(jnp.concatenate(columns, axis=1))
        square[rows, :] = squares
        acc[rows, :] += jnp.dot(
            jnp.concatenate(scaled, axis=1),
            jnp.concatenate(right, axis=0),
            preferred_element_type=jnp.float32,
        )

    def await_gains(offsets):
        for offset in offsets:
            gain_core_copy(at_z(offset), 1 - core).wait_recv()

    def gather_step(layer, step):
        origins = (at_z(-step), at_z(step))
        if layer == 0:
            for direction in range(2):
                if step == steps and direction == 1:
                    continue
                if step > 0:
                    gain_copy(origins[direction], direction, step - 1).wait_recv()
                if step < steps - 1 or (step == steps - 1 and direction == 0):
                    gain_copy(origins[direction], direction, step).start()
                if step > 0 or direction == 0:
                    gain_core_copy(origins[direction], core).start()
        groups = BLOCKS_AT.get((layer, step), ())
        if layer == 0:
            await_gains([offset for group in groups for offset in group])
        for far in (True, False):

            @pl.loop(0 if far else CHUNKS // 2, CHUNKS // 2 if far else CHUNKS)
            def _(slot):
                for direction in range(2):
                    if step == steps and not far:
                        continue
                    chunk = slot if direction == 0 else lax.rem(slot + CHUNKS // 2, CHUNKS)
                    if step > 0:
                        z_copy(layer, origins[direction], chunk, direction, step - 1).wait_recv()
                    if step < steps - 1 or (step == steps - 1 and far):
                        z_copy(layer, origins[direction], chunk, direction, step).start()
                    if step > 0 or direction == 0:
                        core_copy(layer, origins[direction], chunk, core).start()
                for offsets in groups:
                    add_rows(layer, offsets, slot)

    def project(layer):
        mean = jnp.sum(square[...], axis=1, keepdims=True) * (1.0 / features)
        scale = lax.rsqrt(mean + EPS)
        kv[layer, LOW : LOW + TOK, :] = (acc[:, HEAD:] * scale).astype(jnp.bfloat16)
        up, down = halo_copies(layer)
        up.start()
        down.start()
        query[...] = (acc[:, :HEAD] * scale).astype(jnp.bfloat16)

    def halo_copies(layer):
        up = remote(
            kv.at[layer, pl.ds(TOK, LOW)],
            kv.at[layer, pl.ds(0, LOW)],
            halo_send.at[layer, 0],
            halo_recv.at[layer, 0],
            sp_next,
        )
        down = remote(
            kv.at[layer, pl.ds(LOW, HIGH)],
            kv.at[layer, pl.ds(LOW + TOK, HIGH)],
            halo_send.at[layer, 1],
            halo_recv.at[layer, 1],
            sp_prev,
        )
        return up, down

    def scores(layer, chunk, keys, bias, first_row):
        score = lax.dot_general(
            query[chunk_rows(chunk), :],
            kv[layer, keys, 0:HEAD],
            (((1,), (1,)), ((), ())),
            preferred_element_type=jnp.float32,
        )
        grid_rows = PART // GRID_W
        start = chunk * grid_rows - first_row
        band_of = [bias[layer, start + i] for i in range(grid_rows)]
        return score * (HEAD**-0.5) + jnp.concatenate(band_of, axis=0)

    def mix(layer, weight, keys):
        return jnp.dot(
            weight.astype(jnp.bfloat16), kv[layer, keys, HEAD:], preferred_element_type=jnp.float32
        )

    def attend_own(layer, chunk):
        keys = pl.ds(LOW, TOK)
        score = scores(layer, chunk, keys, own_bias, 0)
        most = jnp.max(score, axis=1, keepdims=True)
        weight = jnp.exp(score - most)
        return most, jnp.sum(weight, axis=1, keepdims=True), mix(layer, weight, keys)

    def attend_halo(layer, chunk, own_part):
        most, total, mixed = own_part
        low = chunk < CHUNKS // 2
        keys = pl.ds(0 if low else LOW + TOK, LOW)
        bias, first_row = (low_bias, 0) if low else (high_bias, 4)
        score = scores(layer, chunk, keys, bias, first_row)
        over = jnp.maximum(most, jnp.max(score, axis=1, keepdims=True))
        weight = jnp.exp(score - over)
        kept = jnp.exp(most - over)
        total = total * kept + jnp.sum(weight, axis=1, keepdims=True)
        return (mixed * kept + mix(layer, weight, keys)) / total

    def weight_rounds(layer, at):
        for action, which, name in WEIGHTS_AT.get((layer, at), ()):
            weight_round(action, which, name)

    loads[0].wait()
    for layer in range(2):
        for step in range(steps + 1):
            if layer == 0 or step > 0:
                gather_step(layer, step)
            if layer == 0 and step == 0:
                for load in loads[5:]:
                    load.wait()
            weight_rounds(layer, step)
            if layer == 0 and step == 0:
                for at in range(2):
                    loads[3 + at].wait()
                    build_bias(at)
            if step == 0:
                acc[...] = jnp.zeros_like(acc)
                square[...] = jnp.zeros_like(square)

        if layer == 0:
            await_gains((steps,))

        @pl.loop(0, CHUNKS)
        def _(chunk):
            add_rows(layer, (steps,), chunk)

        project(layer)
        weight_rounds(layer, "halo")
        own_parts = [attend_own(layer, chunk) for chunk in range(CHUNKS)]
        up, down = halo_copies(layer)
        for chunk in range(CHUNKS):
            if chunk == 0:
                up.wait_recv()
            if chunk == CHUNKS // 2:
                down.wait_recv()
            rows = chunk_rows(chunk)
            x = xg[layer, z, core, rows, :].astype(jnp.float32)
            result = (x + attend_halo(layer, chunk, own_parts[chunk])).astype(jnp.bfloat16)
            if layer == 0:
                xg[1, z, core, rows, :] = result
                for direction in range(2):
                    z_copy(1, z, chunk, direction, 0).start()
                core_copy(1, z, chunk, core).start()
            else:
                out[rows, :] = result

    sent = gains.at[pl.ds(0, zn - 1), 0]
    remote(sent, sent, gain_send, gain_recv.at[0, 0], z_next).wait_send()
    sent = gains.at[pl.ds(0, zn), 0]
    remote(sent, sent, gain_core_send, gain_core_recv.at[0], sibling).wait_send()
    for layer in range(2):
        sent = xg.at[layer, pl.ds(0, zn - 1), 0]
        remote(sent, sent, z_send.at[layer], z_recv.at[layer, 0, 0, 0], z_next).wait_send()
        sent = xg.at[layer, pl.ds(0, zn), 0]
        remote(sent, sent, core_send.at[layer], core_recv.at[layer, 0, 0], sibling).wait_send()
        sent = weights.at[layer, pl.ds(0, n_sp - 1)]
        remote(sent, sent, w_send.at[layer], w_recv.at[layer, 0, 0], sp_next).wait_send()
        for copy in halo_copies(layer):
            copy.wait_send()


def body(zn, x, gain0, q0, k0, v0, table0, gain1, q1, k1, v1, table1):
    piece = q0.shape[0] // 4
    pieces = [w.reshape(4, piece, HEAD) for w in (q0, k0, v0, q1, k1, v1)]
    steps = zn // 2
    n_sp = SIDE * SIDE
    hbm = pl.BlockSpec(memory_space=pltpu.HBM)
    vmem = pl.BlockSpec(memory_space=pltpu.VMEM)
    dma = pltpu.SemaphoreType.DMA
    return pl.pallas_call(
        functools.partial(kernel, zn),
        out_shape=jax.ShapeDtypeStruct((TOK, HEAD), jnp.bfloat16),
        in_specs=[hbm] * 11,
        out_specs=vmem,
        scratch_shapes=[
            pltpu.VMEM((2, zn, 2, TOK, HEAD), jnp.bfloat16),
            pltpu.VMEM((2, n_sp, 4, 3, piece, HEAD), jnp.bfloat16),
            pltpu.VMEM((2, LOW + TOK + 4 * GRID_W, 2 * HEAD), jnp.bfloat16),
            pltpu.VMEM((TOK, HEAD), jnp.bfloat16),
            pltpu.VMEM((TOK, 3 * HEAD), jnp.float32),
            pltpu.VMEM((TOK, HEAD), jnp.float32),
            pltpu.VMEM((2, 1, HEAD), jnp.bfloat16),
            pltpu.VMEM((zn, 2, PAD, HEAD), jnp.bfloat16),
            pltpu.VMEM((2, 15, 1, 31), jnp.float32),
            pltpu.VMEM((16, HEAD), jnp.float32),
            pltpu.VMEM((14, GRID_W, HEAD), jnp.float32),
            pltpu.VMEM((2, ROWS, GRID_W, TOK), jnp.float32),
            pltpu.VMEM((2, 4, GRID_W, LOW), jnp.float32),
            pltpu.VMEM((2, 4, GRID_W, LOW), jnp.float32),
            dma((11,)),
            dma((2,)),
            dma((2, 2, steps, CHUNKS)),
            dma((2,)),
            dma((2, zn, CHUNKS)),
            dma,
            dma((2, steps)),
            dma,
            dma((zn,)),
            dma((2,)),
            dma((2, 4, 10)),
            dma((2, 2)),
            dma((2, 2)),
        ],
        compiler_params=pltpu.CompilerParams(
            collective_id=0, has_side_effects=True, vmem_limit_bytes=67043328
        ),
        name="neighbourhood",
    )(
        x,
        gain0.reshape(1, HEAD),
        gain1.reshape(1, HEAD),
        *pieces,
        jnp.swapaxes(table0, 0, 1),
        jnp.swapaxes(table1, 0, 1),
    )


def solution(mesh):
    placed = (
        P("sp", "tp"),
        P("tp"),
        P("sp", "tp"),
        P("sp", "tp"),
        P("sp", "tp"),
        P("tp", None, None),
        P("tp"),
        P("sp", "tp"),
        P("sp", "tp"),
        P("sp", "tp"),
        P("tp", None, None),
    )
    return jax.shard_map(
        functools.partial(body, mesh.shape["tp"] // 2),
        mesh=mesh,
        in_specs=placed,
        out_specs=P("sp", "tp"),
        check_vma=False,
    )
```

time: 109 us -> 93.6 us (0.86)
  Pallas kernels: 101 us -> 91.9 us
  local copies, waits for them, and re-layouts: 7.96 us -> 1.57 us
    pallas_call x1, Pallas kernels: 101 us -> 91.9 us  [body(): pl.pallas_call(functools.partial(kernel, zn), out_shape=jax.ShapeDtypeStr...]
    unnamed x25 -> x1, local copies, waits for them, and re-layouts: 7.96 us -> 1.57 us
where the time goes in v2:
time: 93.6 us; the launch traced here: 93.4 us
  Pallas kernels  91.9 us (98%)
  local copies, waits for them, and re-layouts  1.57 us (2%)
    pallas_call x1, Pallas kernels, body(): pl.pallas_call(functools.partial(kernel, zn), out_shape=jax.ShapeDtypeStr...  91.9 us

profile of v2, /device:TPU:1, one launch (start us, length us, event | category | flops | bytes accessed | tf_op | source)
XLA Modules:
  0.0 93.4 jit_solution(9100747658334911062)
XLA Ops:
  0.0 91.9 %neighbourhood.1 = bf16[512,128]{1,0:T(8,128)(2,1)} custom-call(bf16[512,128]{1,0:T(8,128)(2,1)} %x_hbm.1, bf16[1,128]{1,0:T(2,128)(2,1)} %bitcast.18, bf16[1,128]{1,0:T(2,128)(2,1)} %bitcast.19, bf16[4,64,128]{2,1,0:T(8,128)(2,1)} %bitcast.10, bf16[4,64,128]{2,1,0:T(8,128)(2,1)} %bitcast.11, bf16[4,64,128]{2,1,0:T(8,128)(2,1)} %bitcast.12, ...), custom_call_target="tpu_custom_call" | custom-call | tf_op jit(solution)/shard_map/neighbourhood/pallas_call | solution.py:471
  91.9 1.6 %copy.13 = bf16[512,128]{1,0:T(8,128)(2,1)} copy(bf16[512,128]{1,0:T(8,128)(2,1)} %neighbourhood.1) | data formatting | bytes 262144

commit v3 on v2

v3 whole, which is shorter than its diff:
```python
import functools

import jax
import jax.numpy as jnp
from jax import lax
from jax.experimental import pallas as pl
from jax.experimental.pallas import tpu as pltpu
from jax.sharding import PartitionSpec as P

GRID_W = 64
HEAD = 128
ROWS = 8
TOK = ROWS * GRID_W
CHUNKS = 4
PART = TOK // CHUNKS
PAD = 16
SIDE = 4
EPS = 1e-6
BLOCK = 2 * HEAD
LOW = 4 * GRID_W
HIGH = 3 * GRID_W
X, Y = 0, 1
LINKS = ((X, 1), (X, -1), (Y, 1), (Y, -1))
MESH_ID = pl.DeviceIdType.MESH


def weight_messages(axis, sign):
    part = 0 if sign > 0 else 1
    half = 1 if axis == X else 0
    own_first = 0 if axis == X else 2
    return (
        ("0a", 0, (0, 0), own_first, 2),
        ("0b", 1, (0, 0), 2 - own_first, 2),
        ("1h", 2, (0, -1), 2 * half, 2),
        ("1h", 2, (0, 1), 2 * half, 2),
        ("1s", 3, (-sign, 0), own_first + part, 1),
        ("1b", 4, (-sign, 0), 2 - own_first + part, 1),
        ("2a", 5, (0, 2), 2 * half, 2),
        ("2b", 6, (-sign, -1), 2 * half + part, 1),
        ("2b", 6, (-sign, 1), 2 * half + part, 1),
        ("3", 7, (-sign, 2), 2 * half + part, 1),
    )


WEIGHTS_AT = {
    (0, 0, 7): (("send", 0, "0a"), ("send", 0, "0b")),
    (0, 1, 3): (("wait", 0, "0a"), ("send", 0, "1s"), ("send", 0, "1h")),
    (0, 2, 6): (("wait", 0, "1s"), ("send", 0, "2a"), ("wait", 0, "0b"), ("send", 0, "1b")),
    (0, 4, 0): (("wait", 0, "1h"), ("send", 0, "2b")),
    (0, 4, 6): (("wait", 0, "2a"), ("send", 0, "3")),
    (0, 6, 2): (
        ("wait", 0, "1b"),
        ("wait", 0, "2b"),
        ("wait", 0, "3"),
        ("send", 1, "0a"),
        ("send", 1, "0b"),
    ),
    (0, 8, 2): (("wait", 1, "0a"), ("send", 1, "1s")),
    (0, "halo", 0): (
        ("wait", 1, "1s"),
        ("send", 1, "2a"),
        ("send", 1, "1h"),
        ("wait", 1, "0b"),
        ("send", 1, "1b"),
    ),
    (1, 1, 5): (("wait", 1, "2a"), ("send", 1, "3")),
    (1, 2, 4): (("wait", 1, "1h"), ("send", 1, "2b")),
    (1, 4, 0): (("wait", 1, "1b"), ("wait", 1, "2b"), ("wait", 1, "3")),
}
BLOCKS_AT = {
    (0, 6, 3): (0,),
    (0, 6, 4): (-1, 1),
    (0, 6, 6): (-2, 2),
    (0, 7, 1): (-3, 3),
    (0, 7, 3): (-4, 4),
    (0, 7, 5): (-5, 5),
    (0, 7, 7): (-6, 6),
    (0, 8, 2): (-7, 7),
    (1, 4, 2): (0,),
    (1, 4, 4): (-1, 1),
    (1, 4, 6): (-2, 2),
    (1, 5, 2): (-3, 3),
    (1, 5, 6): (-4, 4),
    (1, 6, 6): (-5, 5),
    (1, 7, 5): (-6, 6),
    (1, 8, 2): (-7, 7),
}
MASKED = -1e30


def kernel(
    zn,
    x_hbm,
    gain0_hbm,
    gain1_hbm,
    q0_hbm,
    k0_hbm,
    v0_hbm,
    q1_hbm,
    k1_hbm,
    v1_hbm,
    table0_hbm,
    table1_hbm,
    out,
    xg,
    weights,
    kv,
    query,
    acc,
    square,
    own_gains,
    gains,
    tables,
    tab,
    band,
    own_bias,
    low_bias,
    high_bias,
    local_sem,
    z_send,
    z_recv,
    core_send,
    core_recv,
    own_recv,
    gain_send,
    gain_recv,
    gain_core_send,
    gain_core_recv,
    w_send,
    w_recv,
    halo_send,
    halo_recv,
):
    sp = lax.axis_index("sp")
    tp = lax.axis_index("tp")
    n_sp = SIDE * SIDE
    gx, gy = lax.rem(sp, SIDE), lax.div(sp, SIDE)
    core, z = lax.rem(tp, 2), lax.div(tp, 2)
    steps = zn // 2
    shards = n_sp // zn
    features = zn * BLOCK

    def at_z(offset):
        return lax.rem(z + offset + zn, zn)

    def chip(z_at, core_at):
        return {"sp": sp, "tp": z_at * 2 + core_at}

    def grid_sp(dx, dy):
        return lax.rem(gy + dy + SIDE, SIDE) * SIDE + lax.rem(gx + dx + SIDE, SIDE)

    def around(axis, along, across):
        along, across = (along + SIDE) % SIDE, (across + SIDE) % SIDE
        return grid_sp(along, across) if axis == X else grid_sp(across, along)

    sibling = chip(z, 1 - core)
    way = 2 * core - 1
    z_onward, z_source = chip(at_z(-way), core), chip(at_z(way), core)
    sp_next = {"sp": lax.rem(sp + 1, n_sp), "tp": tp}
    sp_prev = {"sp": lax.rem(sp + n_sp - 1, n_sp), "tp": tp}

    loads = [
        pltpu.make_async_copy(x_hbm, xg.at[0, z, core], local_sem.at[0]),
        pltpu.make_async_copy(gain0_hbm, own_gains.at[0], local_sem.at[1]),
        pltpu.make_async_copy(gain1_hbm, own_gains.at[1], local_sem.at[2]),
        pltpu.make_async_copy(table0_hbm, tables.at[0], local_sem.at[3]),
        pltpu.make_async_copy(table1_hbm, tables.at[1], local_sem.at[4]),
    ]
    for layer, refs in enumerate(((q0_hbm, k0_hbm, v0_hbm), (q1_hbm, k1_hbm, v1_hbm))):
        for m, ref in enumerate(refs):
            loads.append(
                pltpu.make_async_copy(
                    ref, weights.at[layer, sp, :, m], local_sem.at[5 + 3 * layer + m]
                )
            )
    for load in loads:
        load.start()

    barrier = pltpu.get_barrier_semaphore()
    peers = [z_source, sibling, sp_next, sp_prev]
    peers += [{"sp": around(axis, sign, 0), "tp": tp} for axis, sign in LINKS]
    for peer in peers:
        pl.semaphore_signal(barrier, inc=1, device_id=peer, device_id_type=MESH_ID)

    for layer in range(2):
        kv[layer, :, LOW + TOK + HIGH :, :] = jnp.zeros((2, GRID_W, HEAD), jnp.bfloat16)

    def build_bias(layer):
        lanes = lax.broadcasted_iota(jnp.int32, (GRID_W, HEAD), 1)
        key_column = lanes & (GRID_W - 1)
        column = lax.broadcasted_iota(jnp.int32, (GRID_W, HEAD), 0)
        first_column = jnp.clip(column - 8, 0, GRID_W - 16)
        in_window = (key_column >= first_column) & (key_column < first_column + 16)
        tab[...] = jnp.zeros_like(tab)
        tab[0:15, 0:31] = tables[layer, :, 0, :]
        rows = tab[...]
        both = rows + pltpu.roll(pltpu.roll(rows, 15, 0), GRID_W, 1)
        for offset in range(14):
            spread = jnp.broadcast_to(both[offset : offset + 1], (GRID_W, HEAD))
            shifted = pltpu.roll(spread, HEAD - 15, 1, stride=1, stride_axis=0)
            band[offset] = jnp.where(in_window, shifted, MASKED)
        at_start = jnp.where(sp == 0, 0.0, MASKED)
        at_end = jnp.where(sp == n_sp - 1, 0.0, MASKED)
        not_start = jnp.where(sp == 0, MASKED, 0.0)
        not_end = jnp.where(sp == n_sp - 1, MASKED, 0.0)
        right = lanes >= GRID_W

        def pair(row, key_row, penalties):
            if penalties == (None, None):
                return jnp.full((GRID_W, HEAD), MASKED, jnp.float32)
            values = [MASKED if p is None else p for p in penalties]
            offset = key_row - row + 7
            base = band[offset]
            return base + jnp.where(right, values[1], values[0])

        def inside(row, key_row):
            return row - 4 <= key_row <= row + 3

        for row in range(ROWS):
            for m in range(0, ROWS, 2):
                penalties = tuple(
                    0.0 if inside(row, m + d) else (at_start if row < 4 else at_end)
                    for d in range(2)
                )
                own_bias[layer, row, :, m * GRID_W : (m + 2) * GRID_W] = pair(row, m, penalties)
            for m in range(0, 4, 2):
                lanes_at = slice(m * GRID_W, (m + 2) * GRID_W)
                if row < 4:
                    penalties = tuple(
                        not_start if inside(row, m + d - 4) else None for d in range(2)
                    )
                    low_bias[layer, row, :, lanes_at] = pair(row, m - 4, penalties)
                else:
                    penalties = tuple(not_end if inside(row, m + d + 8) else None for d in range(2))
                    high_bias[layer, row - 4, :, lanes_at] = pair(row, m + 8, penalties)

    pl.semaphore_wait(barrier, len(peers))

    def remote(src, dst, send_sem, recv_sem, device):
        return pltpu.make_async_remote_copy(
            src_ref=src,
            dst_ref=dst,
            send_sem=send_sem,
            recv_sem=recv_sem,
            device_id=device,
            device_id_type=MESH_ID,
        )

    def chunk_rows(chunk):
        start = chunk * PART
        return pl.ds(start if isinstance(chunk, int) else pl.multiple_of(start, PART), PART)

    def z_copy(layer, origin, part, step):
        c, chunk = part
        ref = xg.at[layer, origin, c, chunk_rows(chunk)]
        return remote(ref, ref, z_send.at[layer], z_recv.at[layer, step, c, chunk], z_onward)

    def core_copy(layer, origin, part):
        c, chunk = part
        ref = xg.at[layer, origin, c, chunk_rows(chunk)]
        return remote(ref, ref, core_send.at[layer], core_recv.at[layer, origin], sibling)

    def own_core_copy(layer, part):
        c, chunk = part
        ref = xg.at[layer, z, c, chunk_rows(chunk)]
        return remote(ref, ref, core_send.at[layer], own_recv.at[layer, chunk], sibling)

    own_parts = [(core, chunk) for chunk in range(CHUNKS)]
    other_parts = [(1 - core, chunk) for chunk in range(CHUNKS)]

    def gain_ref(origin, step):
        return gains.at[origin, core] if step == steps else gains.at[origin]

    def gain_copy(origin, step):
        ref = gain_ref(origin, step + 1)
        return remote(ref, ref, gain_send, gain_recv.at[step], z_onward)

    def gain_core_copy(ref, origin):
        return remote(ref, ref, gain_core_send, gain_core_recv.at[origin], sibling)

    def weight_round(action, layer, name):
        for link, (axis, sign) in enumerate(LINKS):
            device = {"sp": around(axis, sign, 0), "tp": tp}
            messages = [m for m in weight_messages(axis, sign) if m[0] == name]
            if action == "send":
                for _, sem, (along, across), piece, pieces in messages:
                    ref = weights.at[layer, around(axis, along, across), pl.ds(piece, pieces)]
                    recv = w_recv.at[layer, link, sem]
                    remote(ref, ref, w_send.at[layer], recv, device).start()
            else:
                for sem in sorted({m[1] for m in messages}):
                    pieces = sum(m[4] for m in messages if m[1] == sem)
                    ref = weights.at[layer, 0, pl.ds(0, pieces)]
                    recv = w_recv.at[layer, link, sem]
                    remote(ref, ref, w_send.at[layer], recv, device).wait_recv()

    def weight_rounds(layer, step, part):
        for action, which, name in WEIGHTS_AT.get((layer, step, part), ()):
            if (action, which, name) == ("send", 0, "0a"):
                for load in loads[5:]:
                    load.wait()
            weight_round(action, which, name)

    def await_sibling(layer, distance):
        origin = at_z(-way * distance)
        block = xg.at[layer, origin]
        if distance == steps:
            block = block.at[1 - core]
        remote(block, block, core_send.at[layer], core_recv.at[layer, origin], sibling).wait_recv()
        if layer == 0:
            ref = gains.at[origin, 1 - core] if distance == steps else gains.at[origin]
            gain_core_copy(ref, origin).wait_recv()

    def add_blocks(layer, offsets):
        distance = abs(offsets[0])
        if distance:
            await_sibling(layer, distance)
        origins = [at_z(offset) for offset in offsets]
        right, factors = [], []
        for origin in origins:
            columns = []
            for m in range(3):
                pieces = weights[layer, pl.ds(origin * shards, shards), :, m]
                columns.append(pieces.reshape(BLOCK, HEAD))
            right.append(jnp.concatenate(columns, axis=1))
            for c in range(2):
                factors.append(gains[origin, c].astype(jnp.float32)[layer : layer + 1])
        right = jnp.concatenate(right, axis=0)
        for top in range(0, TOK, 256):
            rows = slice(top, top + 256)
            squares, scaled = square[rows, :], []
            for i, origin in enumerate(origins):
                for c in range(2):
                    wide = xg[layer, origin, c, rows, :].astype(jnp.float32)
                    squares = squares + wide * wide
                    scaled.append((wide * factors[2 * i + c]).astype(jnp.bfloat16))
            square[rows, :] = squares
            acc[rows, :] += jnp.dot(
                jnp.concatenate(scaled, axis=1), right, preferred_element_type=jnp.float32
            )

    def own_gain_rows():
        loads[1].wait()
        loads[2].wait()
        spare = jnp.zeros((PAD - 2, HEAD), jnp.float32)
        both_gains = [own_gains[layer].astype(jnp.float32) for layer in range(2)]
        gains[z, core] = jnp.concatenate(both_gains + [spare]).astype(jnp.bfloat16)

    def gather_step(layer, step):
        origin = at_z(way * step)
        if step == 0 and layer == 0:
            for part in own_parts:
                z_copy(layer, z, part, 0).start()
                own_core_copy(layer, part).start()
        if layer == 0:
            if step == 0:
                own_gain_rows()
                gain_core_copy(gains.at[z, core], z).start()
                gain_core_copy(gains.at[z, 1 - core], z).wait_recv()
            else:
                gain_copy(origin, step - 1).wait_recv()
                gain_core_copy(gain_ref(origin, step), origin).start()
            if step < steps:
                gain_copy(origin, step).start()
        for index, part in enumerate(own_parts + other_parts):
            if step == 0:
                if index >= CHUNKS:
                    own_core_copy(layer, part).wait_recv()
                    z_copy(layer, z, part, 0).start()
            elif step < steps or index < CHUNKS:
                z_copy(layer, origin, part, step - 1).wait_recv()
                if step < steps - 1 or (step == steps - 1 and index < CHUNKS):
                    z_copy(layer, origin, part, step).start()
                core_copy(layer, origin, part).start()
            weight_rounds(layer, step, index)
            if (layer, step, index) in BLOCKS_AT:
                add_blocks(layer, BLOCKS_AT[layer, step, index])

    def project(layer):
        mean = jnp.sum(square[...], axis=1, keepdims=True) * (1.0 / features)
        scale = lax.rsqrt(mean + EPS)
        up, down = halo_copies(layer)
        for kind in range(2):
            part = acc[:, (1 + kind) * HEAD : (2 + kind) * HEAD]
            kv[layer, kind, LOW : LOW + TOK, :] = (part * scale).astype(jnp.bfloat16)
            if kind == 0:
                up[0].start()
                down[0].start()
        query[...] = (acc[:, :HEAD] * scale).astype(jnp.bfloat16)

    def halo_copies(layer):
        up, down = [], []
        for kind in range(2):
            both = kv.at[layer, kind]
            up.append(
                remote(
                    both.at[pl.ds(TOK, LOW)],
                    both.at[pl.ds(0, LOW)],
                    halo_send.at[layer, 0, kind],
                    halo_recv.at[layer, 0, kind],
                    sp_next,
                )
            )
            down.append(
                remote(
                    both.at[pl.ds(LOW, HIGH)],
                    both.at[pl.ds(LOW + TOK, HIGH)],
                    halo_send.at[layer, 1, kind],
                    halo_recv.at[layer, 1, kind],
                    sp_prev,
                )
            )
        return up, down

    def scores(layer, half, keys, bands):
        score = lax.dot_general(
            query[pl.ds(half * TOK // 2, TOK // 2), :],
            kv[layer, 0, keys, :],
            (((1,), (1,)), ((), ())),
            preferred_element_type=jnp.float32,
        )
        return score * (HEAD**-0.5) + jnp.concatenate(bands, axis=0)

    def mix(layer, weight, keys):
        return jnp.dot(
            weight.astype(jnp.bfloat16), kv[layer, 1, keys, :], preferred_element_type=jnp.float32
        )

    def attend_own(layer, half):
        keys = pl.ds(LOW, TOK)
        score = scores(layer, half, keys, [own_bias[layer, 4 * half + i] for i in range(4)])
        most = jnp.max(score, axis=1, keepdims=True)
        weight = jnp.exp(score - most)
        return most, jnp.sum(weight, axis=1, keepdims=True), mix(layer, weight, keys)

    def halo_keys(half):
        return pl.ds(0 if half == 0 else LOW + TOK, LOW)

    def halo_weights(layer, half, most):
        bias = low_bias if half == 0 else high_bias
        score = scores(layer, half, halo_keys(half), [bias[layer, i] for i in range(4)])
        over = jnp.maximum(most, jnp.max(score, axis=1, keepdims=True))
        return jnp.exp(score - over), jnp.exp(most - over)

    loads[0].wait()
    for layer in range(2):
        if layer == 1:
            acc[...] = jnp.zeros_like(acc)
            square[...] = jnp.zeros_like(square)
        for step in range(steps + 1):
            gather_step(layer, step)
            if layer == 0 and step == 0:
                for at in range(2):
                    loads[3 + at].wait()
                    build_bias(at)
                acc[...] = jnp.zeros_like(acc)
                square[...] = jnp.zeros_like(square)
        add_blocks(layer, (steps,))
        project(layer)
        halos = halo_copies(layer)
        own = [attend_own(layer, 0)]
        for halo in halos:
            halo[1].start()
        weight_rounds(layer, "halo", 0)
        own.append(attend_own(layer, 1))
        for halo in halos:
            halo[0].wait_recv()
        added = [halo_weights(layer, half, own[half][0]) for half in range(2)]
        for halo in halos:
            halo[1].wait_recv()
        for half in range(2):
            _, total, mixed = own[half]
            weight, kept = added[half]
            total = total * kept + jnp.sum(weight, axis=1, keepdims=True)
            attended = (mixed * kept + mix(layer, weight, halo_keys(half))) / total
            rows = pl.ds(half * TOK // 2, TOK // 2)
            x = xg[layer, z, core, rows, :].astype(jnp.float32)
            result = (x + attended).astype(jnp.bfloat16)
            if layer == 0:
                xg[1, z, core, rows, :] = result
                for part in own_parts[half * CHUNKS // 2 : (half + 1) * CHUNKS // 2]:
                    z_copy(1, z, part, 0).start()
                    own_core_copy(1, part).start()
            else:
                out[rows, :] = result

    sent = gains.at[pl.ds(0, zn - 1), 0]
    remote(sent, sent, gain_send, gain_recv.at[0], z_onward).wait_send()
    sent = gains.at[pl.ds(0, zn), 0]
    remote(sent, sent, gain_core_send, gain_core_recv.at[0], sibling).wait_send()
    for layer in range(2):
        sent = xg.at[layer, pl.ds(0, zn - 1), 0]
        remote(sent, sent, z_send.at[layer], z_recv.at[layer, 0, 0, 0], z_onward).wait_send()
        sent = xg.at[layer, pl.ds(0, zn), 0]
        remote(sent, sent, core_send.at[layer], core_recv.at[layer, 0], sibling).wait_send()
        sent = weights.at[layer, pl.ds(0, n_sp - 1)]
        remote(sent, sent, w_send.at[layer], w_recv.at[layer, 0, 0], sp_next).wait_send()
        for pair in halo_copies(layer):
            for copy in pair:
                copy.wait_send()


def body(zn, x, gain0, q0, k0, v0, table0, gain1, q1, k1, v1, table1):
    piece = q0.shape[0] // 4
    pieces = [w.reshape(4, piece, HEAD) for w in (q0, k0, v0, q1, k1, v1)]
    steps = zn // 2
    n_sp = SIDE * SIDE
    hbm = pl.BlockSpec(memory_space=pltpu.HBM)
    vmem = pl.BlockSpec(memory_space=pltpu.VMEM)
    dma = pltpu.SemaphoreType.DMA
    return pl.pallas_call(
        functools.partial(kernel, zn),
        out_shape=jax.ShapeDtypeStruct((TOK, HEAD), jnp.bfloat16),
        in_specs=[hbm] * 11,
        out_specs=vmem,
        scratch_shapes=[
            pltpu.VMEM((2, zn, 2, TOK, HEAD), jnp.bfloat16),
            pltpu.VMEM((2, n_sp, 4, 3, piece, HEAD), jnp.bfloat16),
            pltpu.VMEM((2, 2, LOW + TOK + 4 * GRID_W, HEAD), jnp.bfloat16),
            pltpu.VMEM((TOK, HEAD), jnp.bfloat16),
            pltpu.VMEM((TOK, 3 * HEAD), jnp.float32),
            pltpu.VMEM((TOK, HEAD), jnp.float32),
            pltpu.VMEM((2, 1, HEAD), jnp.bfloat16),
            pltpu.VMEM((zn, 2, PAD, HEAD), jnp.bfloat16),
            pltpu.VMEM((2, 15, 1, 31), jnp.float32),
            pltpu.VMEM((16, HEAD), jnp.float32),
            pltpu.VMEM((14, GRID_W, HEAD), jnp.float32),
            pltpu.VMEM((2, ROWS, GRID_W, TOK), jnp.float32),
            pltpu.VMEM((2, 4, GRID_W, LOW), jnp.float32),
            pltpu.VMEM((2, 4, GRID_W, LOW), jnp.float32),
            dma((11,)),
            dma((2,)),
            dma((2, steps, 2, CHUNKS)),
            dma((2,)),
            dma((2, zn)),
            dma((2, CHUNKS)),
            dma,
            dma((steps,)),
            dma,
            dma((zn,)),
            dma((2,)),
            dma((2, 4, 8)),
            dma((2, 2, 2)),
            dma((2, 2, 2)),
        ],
        compiler_params=pltpu.CompilerParams(
            collective_id=0, has_side_effects=True, vmem_limit_bytes=67043328
        ),
        name="neighbourhood",
    )(
        x,
        gain0.reshape(1, HEAD),
        gain1.reshape(1, HEAD),
        *pieces,
        jnp.swapaxes(table0, 0, 1),
        jnp.swapaxes(table1, 0, 1),
    )


def solution(mesh):
    placed = (
        P("sp", "tp"),
        P("tp"),
        P("sp", "tp"),
        P("sp", "tp"),
        P("sp", "tp"),
        P("tp", None, None),
        P("tp"),
        P("sp", "tp"),
        P("sp", "tp"),
        P("sp", "tp"),
        P("tp", None, None),
    )
    return jax.shard_map(
        functools.partial(body, mesh.shape["tp"] // 2),
        mesh=mesh,
        in_specs=placed,
        out_specs=P("sp", "tp"),
        check_vma=False,
    )
```

time: 93.6 us -> 87.7 us (0.937)
  Pallas kernels: 91.9 us -> 85.9 us
    pallas_call x1, Pallas kernels: 91.9 us -> 85.9 us  [body(): pl.pallas_call(functools.partial(kernel, zn), out_shape=jax.ShapeDtypeStr...]
where the time goes in v3:
time: 87.7 us; the launch traced here: 87.5 us
  Pallas kernels  85.9 us (98%)
  local copies, waits for them, and re-layouts  1.57 us (2%)
    pallas_call x1, Pallas kernels, body(): pl.pallas_call(functools.partial(kernel, zn), out_shape=jax.ShapeDtypeStr...  85.9 us

profile of v3, /device:TPU:1, one launch (start us, length us, event | category | flops | bytes accessed | tf_op | source)
XLA Modules:
  0.0 87.5 jit_solution(18260359470717763209)
XLA Ops:
  0.0 85.9 %neighbourhood.1 = bf16[512,128]{1,0:T(8,128)(2,1)} custom-call(bf16[512,128]{1,0:T(8,128)(2,1)} %x_hbm.1, bf16[1,128]{1,0:T(2,128)(2,1)} %bitcast.18, bf16[1,128]{1,0:T(2,128)(2,1)} %bitcast.19, bf16[4,64,128]{2,1,0:T(8,128)(2,1)} %bitcast.10, bf16[4,64,128]{2,1,0:T(8,128)(2,1)} %bitcast.11, bf16[4,64,128]{2,1,0:T(8,128)(2,1)} %bitcast.12, ...), custom_call_target="tpu_custom_call" | custom-call | tf_op jit(solution)/shard_map/neighbourhood/pallas_call | solution.py:511
  85.9 1.6 %copy.13 = bf16[512,128]{1,0:T(8,128)(2,1)} copy(bf16[512,128]{1,0:T(8,128)(2,1)} %neighbourhood.1) | data formatting | bytes 262144

commit v4 on v3

--- a/solution.py
+++ b/solution.py
@@ -34,28 +34,23 @@
         ("1h", 2, (0, -1), 2 * half, 2),
         ("1h", 2, (0, 1), 2 * half, 2),
         ("1s", 3, (-sign, 0), own_first + part, 1),
-        ("1b", 4, (-sign, 0), 2 - own_first + part, 1),
-        ("2a", 5, (0, 2), 2 * half, 2),
-        ("2b", 6, (-sign, -1), 2 * half + part, 1),
-        ("2b", 6, (-sign, 1), 2 * half + part, 1),
-        ("3", 7, (-sign, 2), 2 * half + part, 1),
+        ("1b", 5, (-sign, 0), 2 - own_first + part, 1),
+        ("2a", 4, (0, 2), 2 * half, 2),
+        ("2b", 5, (-sign, -1), 2 * half + part, 1),
+        ("2b", 5, (-sign, 1), 2 * half + part, 1),
+        ("3", 5, (-sign, 2), 2 * half + part, 1),
     )
 
 
 WEIGHTS_AT = {
     (0, 0, 7): (("send", 0, "0a"), ("send", 0, "0b")),
-    (0, 1, 3): (("wait", 0, "0a"), ("send", 0, "1s"), ("send", 0, "1h")),
-    (0, 2, 6): (("wait", 0, "1s"), ("send", 0, "2a"), ("wait", 0, "0b"), ("send", 0, "1b")),
-    (0, 4, 0): (("wait", 0, "1h"), ("send", 0, "2b")),
-    (0, 4, 6): (("wait", 0, "2a"), ("send", 0, "3")),
-    (0, 6, 2): (
-        ("wait", 0, "1b"),
-        ("wait", 0, "2b"),
-        ("wait", 0, "3"),
-        ("send", 1, "0a"),
-        ("send", 1, "0b"),
-    ),
-    (0, 8, 2): (("wait", 1, "0a"), ("send", 1, "1s")),
+    (0, 1, 3): (("wait", 0, "0a"), ("send", 0, "1s")),
+    (0, 1, 5): (("send", 0, "1h"),),
+    (0, 3, 0): (("wait", 0, "1s"), ("send", 0, "2a")),
+    (0, 4, 3): (("wait", 0, "1h"), ("send", 0, "2b"), ("wait", 0, "0b"), ("send", 0, "1b")),
+    (0, 5, 1): (("wait", 0, "2a"), ("send", 0, "3")),
+    (0, 6, 5): (("wait", 0, "3"), ("send", 1, "0a"), ("send", 1, "0b")),
+    (0, 8, 3): (("wait", 1, "0a"), ("send", 1, "1s")),
     (0, "halo", 0): (
         ("wait", 1, "1s"),
         ("send", 1, "2a"),
@@ -64,26 +59,26 @@
         ("send", 1, "1b"),
     ),
     (1, 1, 5): (("wait", 1, "2a"), ("send", 1, "3")),
-    (1, 2, 4): (("wait", 1, "1h"), ("send", 1, "2b")),
-    (1, 4, 0): (("wait", 1, "1b"), ("wait", 1, "2b"), ("wait", 1, "3")),
+    (1, 3, 1): (("wait", 1, "1h"), ("send", 1, "2b")),
+    (1, 5, 0): (("wait", 1, "3"),),
 }
 BLOCKS_AT = {
-    (0, 6, 3): (0,),
-    (0, 6, 4): (-1, 1),
-    (0, 6, 6): (-2, 2),
+    (0, 6, 6): (0,),
+    (0, 6, 7): (-1, 1),
+    (0, 7, 0): (-2, 2),
     (0, 7, 1): (-3, 3),
     (0, 7, 3): (-4, 4),
     (0, 7, 5): (-5, 5),
     (0, 7, 7): (-6, 6),
     (0, 8, 2): (-7, 7),
-    (1, 4, 2): (0,),
-    (1, 4, 4): (-1, 1),
-    (1, 4, 6): (-2, 2),
-    (1, 5, 2): (-3, 3),
-    (1, 5, 6): (-4, 4),
+    (1, 5, 1): (0,),
+    (1, 5, 2): (-1, 1),
+    (1, 5, 4): (-2, 2),
+    (1, 5, 6): (-3, 3),
+    (1, 6, 2): (-4, 4),
     (1, 6, 6): (-5, 5),
     (1, 7, 5): (-6, 6),
-    (1, 8, 2): (-7, 7),
+    (1, 8, 3): (-7, 7),
 }
 MASKED = -1e30
 
@@ -116,6 +111,7 @@
     own_bias,
     low_bias,
     high_bias,
+    result_buffer,
     local_sem,
     z_send,
     z_recv,
@@ -159,6 +155,12 @@
     sp_next = {"sp": lax.rem(sp + 1, n_sp), "tp": tp}
     sp_prev = {"sp": lax.rem(sp + n_sp - 1, n_sp), "tp": tp}
 
+    barrier = pltpu.get_barrier_semaphore()
+    peers = [z_source, sibling, sp_next, sp_prev]
+    peers += [{"sp": around(axis, sign, 0), "tp": tp} for axis, sign in LINKS]
+    for peer in peers:
+        pl.semaphore_signal(barrier, inc=1, device_id=peer, device_id_type=MESH_ID)
+
     loads = [
         pltpu.make_async_copy(x_hbm, xg.at[0, z, core], local_sem.at[0]),
         pltpu.make_async_copy(gain0_hbm, own_gains.at[0], local_sem.at[1]),
@@ -175,12 +177,6 @@
             )
     for load in loads:
         load.start()
-
-    barrier = pltpu.get_barrier_semaphore()
-    peers = [z_source, sibling, sp_next, sp_prev]
-    peers += [{"sp": around(axis, sign, 0), "tp": tp} for axis, sign in LINKS]
-    for peer in peers:
-        pl.semaphore_signal(barrier, inc=1, device_id=peer, device_id_type=MESH_ID)
 
     for layer in range(2):
         kv[layer, :, LOW + TOK + HIGH :, :] = jnp.zeros((2, GRID_W, HEAD), jnp.bfloat16)
@@ -281,18 +277,19 @@
     def weight_round(action, layer, name):
         for link, (axis, sign) in enumerate(LINKS):
             device = {"sp": around(axis, sign, 0), "tp": tp}
-            messages = [m for m in weight_messages(axis, sign) if m[0] == name]
+            messages = weight_messages(axis, sign)
             if action == "send":
+                messages = [m for m in messages if m[0] == name]
                 for _, sem, (along, across), piece, pieces in messages:
                     ref = weights.at[layer, around(axis, along, across), pl.ds(piece, pieces)]
                     recv = w_recv.at[layer, link, sem]
                     remote(ref, ref, w_send.at[layer], recv, device).start()
             else:
-                for sem in sorted({m[1] for m in messages}):
-                    pieces = sum(m[4] for m in messages if m[1] == sem)
-                    ref = weights.at[layer, 0, pl.ds(0, pieces)]
-                    recv = w_recv.at[layer, link, sem]
-                    remote(ref, ref, w_send.at[layer], recv, device).wait_recv()
+                (sem,) = {m[1] for m in messages if m[0] == name}
+                pieces = sum(m[4] for m in messages if m[1] == sem)
+                ref = weights.at[layer, 0, pl.ds(0, pieces)]
+                recv = w_recv.at[layer, link, sem]
+                remote(ref, ref, w_send.at[layer], recv, device).wait_recv()
 
     def weight_rounds(layer, step, part):
         for action, which, name in WEIGHTS_AT.get((layer, step, part), ()):
@@ -379,37 +376,30 @@
     def project(layer):
         mean = jnp.sum(square[...], axis=1, keepdims=True) * (1.0 / features)
         scale = lax.rsqrt(mean + EPS)
-        up, down = halo_copies(layer)
         for kind in range(2):
             part = acc[:, (1 + kind) * HEAD : (2 + kind) * HEAD]
             kv[layer, kind, LOW : LOW + TOK, :] = (part * scale).astype(jnp.bfloat16)
             if kind == 0:
-                up[0].start()
-                down[0].start()
+                for halo in halo_copies(layer, 0):
+                    halo.start()
         query[...] = (acc[:, :HEAD] * scale).astype(jnp.bfloat16)
 
-    def halo_copies(layer):
-        up, down = [], []
-        for kind in range(2):
-            both = kv.at[layer, kind]
-            up.append(
-                remote(
-                    both.at[pl.ds(TOK, LOW)],
-                    both.at[pl.ds(0, LOW)],
-                    halo_send.at[layer, 0, kind],
-                    halo_recv.at[layer, 0, kind],
-                    sp_next,
-                )
-            )
-            down.append(
-                remote(
-                    both.at[pl.ds(LOW, HIGH)],
-                    both.at[pl.ds(LOW + TOK, HIGH)],
-                    halo_send.at[layer, 1, kind],
-                    halo_recv.at[layer, 1, kind],
-                    sp_prev,
-                )
-            )
+    def halo_copies(layer, kind):
+        both = kv.at[layer, kind]
+        up = remote(
+            both.at[pl.ds(TOK, LOW)],
+            both.at[pl.ds(0, LOW)],
+            halo_send.at[layer, 0, kind],
+            halo_recv.at[layer, 0, kind],
+            sp_next,
+        )
+        down = remote(
+            both.at[pl.ds(LOW, HIGH)],
+            both.at[pl.ds(LOW + TOK, HIGH)],
+            halo_send.at[layer, 1, kind],
+            halo_recv.at[layer, 1, kind],
+            sp_prev,
+        )
         return up, down
 
     def scores(layer, half, keys, bands):
@@ -441,6 +431,15 @@
         score = scores(layer, half, halo_keys(half), [bias[layer, i] for i in range(4)])
         over = jnp.maximum(most, jnp.max(score, axis=1, keepdims=True))
         return jnp.exp(score - over), jnp.exp(most - over)
+
+    outs = [
+        pltpu.make_async_copy(
+            result_buffer.at[pl.ds(half * TOK // 2, TOK // 2)],
+            out.at[pl.ds(half * TOK // 2, TOK // 2)],
+            local_sem.at[11 + half],
+        )
+        for half in range(2)
+    ]
 
     loads[0].wait()
     for layer in range(2):
@@ -457,17 +456,16 @@
                 square[...] = jnp.zeros_like(square)
         add_blocks(layer, (steps,))
         project(layer)
-        halos = halo_copies(layer)
         own = [attend_own(layer, 0)]
-        for halo in halos:
-            halo[1].start()
+        for halo in halo_copies(layer, 1):
+            halo.start()
+        own.append(attend_own(layer, 1))
+        for halo in halo_copies(layer, 0):
+            halo.wait_recv()
         weight_rounds(layer, "halo", 0)
-        own.append(attend_own(layer, 1))
-        for halo in halos:
-            halo[0].wait_recv()
         added = [halo_weights(layer, half, own[half][0]) for half in range(2)]
-        for halo in halos:
-            halo[1].wait_recv()
+        for halo in halo_copies(layer, 1):
+            halo.wait_recv()
         for half in range(2):
             _, total, mixed = own[half]
             weight, kept = added[half]
@@ -482,8 +480,11 @@
                     z_copy(1, z, part, 0).start()
                     own_core_copy(1, part).start()
             else:
-                out[rows, :] = result
-
+                result_buffer[rows, :] = result
+                outs[half].start()
+
+    for copy in outs:
+        copy.wait()
     sent = gains.at[pl.ds(0, zn - 1), 0]
     remote(sent, sent, gain_send, gain_recv.at[0], z_onward).wait_send()
     sent = gains.at[pl.ds(0, zn), 0]
@@ -495,9 +496,9 @@
         remote(sent, sent, core_send.at[layer], core_recv.at[layer, 0], sibling).wait_send()
         sent = weights.at[layer, pl.ds(0, n_sp - 1)]
         remote(sent, sent, w_send.at[layer], w_recv.at[layer, 0, 0], sp_next).wait_send()
-        for pair in halo_copies(layer):
-            for copy in pair:
-                copy.wait_send()
+        for kind in range(2):
+            for halo in halo_copies(layer, kind):
+                halo.wait_send()
 
 
 def body(zn, x, gain0, q0, k0, v0, table0, gain1, q1, k1, v1, table1):
@@ -506,13 +507,12 @@
     steps = zn // 2
     n_sp = SIDE * SIDE
     hbm = pl.BlockSpec(memory_space=pltpu.HBM)
-    vmem = pl.BlockSpec(memory_space=pltpu.VMEM)
     dma = pltpu.SemaphoreType.DMA
     return pl.pallas_call(
         functools.partial(kernel, zn),
         out_shape=jax.ShapeDtypeStruct((TOK, HEAD), jnp.bfloat16),
         in_specs=[hbm] * 11,
-        out_specs=vmem,
+        out_specs=hbm,
         scratch_shapes=[
             pltpu.VMEM((2, zn, 2, TOK, HEAD), jnp.bfloat16),
             pltpu.VMEM((2, n_sp, 4, 3, piece, HEAD), jnp.bfloat16),
@@ -528,7 +528,8 @@
             pltpu.VMEM((2, ROWS, GRID_W, TOK), jnp.float32),
             pltpu.VMEM((2, 4, GRID_W, LOW), jnp.float32),
             pltpu.VMEM((2, 4, GRID_W, LOW), jnp.float32),
-            dma((11,)),
+            pltpu.VMEM((TOK, HEAD), jnp.bfloat16),
+            dma((13,)),
             dma((2,)),
             dma((2, steps, 2, CHUNKS)),
             dma((2,)),
@@ -539,7 +540,7 @@
             dma,
             dma((zn,)),
             dma((2,)),
-            dma((2, 4, 8)),
+            dma((2, 4, 6)),
             dma((2, 2, 2)),
             dma((2, 2, 2)),
         ],

time: 87.7 us -> 86.7 us (0.989)
  Pallas kernels: 85.9 us -> 85 us
    pallas_call x1, Pallas kernels: 85.9 us -> 85 us  [body(): pl.pallas_call(functools.partial(kernel, zn), out_shape=jax.ShapeDtypeStr...]
where the time goes in v4:
time: 86.7 us; the launch traced here: 86.5 us
  Pallas kernels  85 us (98%)
  local copies, waits for them, and re-layouts  1.57 us (2%)
    pallas_call x1, Pallas kernels, body(): pl.pallas_call(functools.partial(kernel, zn), out_shape=jax.ShapeDtypeStr...  85 us

profile of v4, /device:TPU:1, one launch (start us, length us, event | category | flops | bytes accessed | tf_op | source)
XLA Modules:
  0.0 86.5 jit_solution(11102426576371680241)
XLA Ops:
  0.0 85.0 %neighbourhood.1 = bf16[512,128]{1,0:T(8,128)(2,1)} custom-call(bf16[512,128]{1,0:T(8,128)(2,1)} %x_hbm.1, bf16[1,128]{1,0:T(2,128)(2,1)} %bitcast.18, bf16[1,128]{1,0:T(2,128)(2,1)} %bitcast.19, bf16[4,64,128]{2,1,0:T(8,128)(2,1)} %bitcast.10, bf16[4,64,128]{2,1,0:T(8,128)(2,1)} %bitcast.11, bf16[4,64,128]{2,1,0:T(8,128)(2,1)} %bitcast.12, ...), custom_call_target="tpu_custom_call" | custom-call | tf_op jit(solution)/shard_map/neighbourhood/pallas_call | solution.py:511
  85.0 1.6 %copy.13 = bf16[512,128]{1,0:T(8,128)(2,1)} copy(bf16[512,128]{1,0:T(8,128)(2,1)} %neighbourhood.1) | data formatting | bytes 262144

commit v5 on v4

--- a/solution.py
+++ b/solution.py
@@ -64,21 +64,21 @@
 }
 BLOCKS_AT = {
     (0, 6, 6): (0,),
-    (0, 6, 7): (-1, 1),
-    (0, 7, 0): (-2, 2),
-    (0, 7, 1): (-3, 3),
-    (0, 7, 3): (-4, 4),
-    (0, 7, 5): (-5, 5),
+    (0, 7, 0): (-1, 1),
+    (0, 7, 3): (-2, 2),
+    (0, 7, 4): (-3, 3),
+    (0, 7, 5): (-4, 4),
+    (0, 7, 6): (-5, 5),
     (0, 7, 7): (-6, 6),
-    (0, 8, 2): (-7, 7),
-    (1, 5, 1): (0,),
-    (1, 5, 2): (-1, 1),
-    (1, 5, 4): (-2, 2),
-    (1, 5, 6): (-3, 3),
-    (1, 6, 2): (-4, 4),
-    (1, 6, 6): (-5, 5),
-    (1, 7, 5): (-6, 6),
-    (1, 8, 3): (-7, 7),
+    (0, 8, 1): (-7, 7),
+    (1, 5, 3): (0,),
+    (1, 5, 6): (-1, 1),
+    (1, 6, 1): (-2, 2),
+    (1, 6, 5): (-3, 3),
+    (1, 7, 3): (-4, 4),
+    (1, 7, 4): (-5, 5),
+    (1, 7, 6): (-6, 6),
+    (1, 8, 1): (-7, 7),
 }
 MASKED = -1e30
 
@@ -111,13 +111,13 @@
     own_bias,
     low_bias,
     high_bias,
-    result_buffer,
     local_sem,
     z_send,
     z_recv,
     core_send,
     core_recv,
     own_recv,
+    next_layer,
     gain_send,
     gain_recv,
     gain_core_send,
@@ -249,17 +249,17 @@
     def z_copy(layer, origin, part, step):
         c, chunk = part
         ref = xg.at[layer, origin, c, chunk_rows(chunk)]
-        return remote(ref, ref, z_send.at[layer], z_recv.at[layer, step, c, chunk], z_onward)
+        return remote(ref, ref, z_send.at[layer], z_recv.at[step, c, chunk], z_onward)
 
     def core_copy(layer, origin, part):
         c, chunk = part
         ref = xg.at[layer, origin, c, chunk_rows(chunk)]
-        return remote(ref, ref, core_send.at[layer], core_recv.at[layer, origin], sibling)
+        return remote(ref, ref, core_send.at[layer], core_recv.at[origin], sibling)
 
     def own_core_copy(layer, part):
         c, chunk = part
         ref = xg.at[layer, z, c, chunk_rows(chunk)]
-        return remote(ref, ref, core_send.at[layer], own_recv.at[layer, chunk], sibling)
+        return remote(ref, ref, core_send.at[layer], own_recv.at[chunk], sibling)
 
     own_parts = [(core, chunk) for chunk in range(CHUNKS)]
     other_parts = [(1 - core, chunk) for chunk in range(CHUNKS)]
@@ -303,7 +303,7 @@
         block = xg.at[layer, origin]
         if distance == steps:
             block = block.at[1 - core]
-        remote(block, block, core_send.at[layer], core_recv.at[layer, origin], sibling).wait_recv()
+        remote(block, block, core_send.at[layer], core_recv.at[origin], sibling).wait_recv()
         if layer == 0:
             ref = gains.at[origin, 1 - core] if distance == steps else gains.at[origin]
             gain_core_copy(ref, origin).wait_recv()
@@ -432,15 +432,6 @@
         over = jnp.maximum(most, jnp.max(score, axis=1, keepdims=True))
         return jnp.exp(score - over), jnp.exp(most - over)
 
-    outs = [
-        pltpu.make_async_copy(
-            result_buffer.at[pl.ds(half * TOK // 2, TOK // 2)],
-            out.at[pl.ds(half * TOK // 2, TOK // 2)],
-            local_sem.at[11 + half],
-        )
-        for half in range(2)
-    ]
-
     loads[0].wait()
     for layer in range(2):
         if layer == 1:
@@ -455,6 +446,11 @@
                 acc[...] = jnp.zeros_like(acc)
                 square[...] = jnp.zeros_like(square)
         add_blocks(layer, (steps,))
+        if layer == 0:
+            for index, device in enumerate((z_source, sibling)):
+                pl.semaphore_signal(
+                    next_layer.at[index], inc=1, device_id=device, device_id_type=MESH_ID
+                )
         project(layer)
         own = [attend_own(layer, 0)]
         for halo in halo_copies(layer, 1):
@@ -476,24 +472,24 @@
             result = (x + attended).astype(jnp.bfloat16)
             if layer == 0:
                 xg[1, z, core, rows, :] = result
+                if half == 0:
+                    for index in range(2):
+                        pl.semaphore_wait(next_layer.at[index], 1)
                 for part in own_parts[half * CHUNKS // 2 : (half + 1) * CHUNKS // 2]:
                     z_copy(1, z, part, 0).start()
                     own_core_copy(1, part).start()
             else:
-                result_buffer[rows, :] = result
-                outs[half].start()
-
-    for copy in outs:
-        copy.wait()
+                out[rows, :] = result
+
     sent = gains.at[pl.ds(0, zn - 1), 0]
     remote(sent, sent, gain_send, gain_recv.at[0], z_onward).wait_send()
     sent = gains.at[pl.ds(0, zn), 0]
     remote(sent, sent, gain_core_send, gain_core_recv.at[0], sibling).wait_send()
     for layer in range(2):
         sent = xg.at[layer, pl.ds(0, zn - 1), 0]
-        remote(sent, sent, z_send.at[layer], z_recv.at[layer, 0, 0, 0], z_onward).wait_send()
+        remote(sent, sent, z_send.at[layer], z_recv.at[0, 0, 0], z_onward).wait_send()
         sent = xg.at[layer, pl.ds(0, zn), 0]
-        remote(sent, sent, core_send.at[layer], core_recv.at[layer, 0], sibling).wait_send()
+        remote(sent, sent, core_send.at[layer], core_recv.at[0], sibling).wait_send()
         sent = weights.at[layer, pl.ds(0, n_sp - 1)]
         remote(sent, sent, w_send.at[layer], w_recv.at[layer, 0, 0], sp_next).wait_send()
         for kind in range(2):
@@ -510,9 +506,9 @@
     dma = pltpu.SemaphoreType.DMA
     return pl.pallas_call(
         functools.partial(kernel, zn),
-        out_shape=jax.ShapeDtypeStruct((TOK, HEAD), jnp.bfloat16),
+        out_shape=pltpu.VMEM((TOK, HEAD), jnp.bfloat16),
         in_specs=[hbm] * 11,
-        out_specs=hbm,
+        out_specs=pl.BlockSpec(memory_space=pltpu.VMEM),
         scratch_shapes=[
             pltpu.VMEM((2, zn, 2, TOK, HEAD), jnp.bfloat16),
             pltpu.VMEM((2, n_sp, 4, 3, piece, HEAD), jnp.bfloat16),
@@ -528,13 +524,13 @@
             pltpu.VMEM((2, ROWS, GRID_W, TOK), jnp.float32),
             pltpu.VMEM((2, 4, GRID_W, LOW), jnp.float32),
             pltpu.VMEM((2, 4, GRID_W, LOW), jnp.float32),
-            pltpu.VMEM((TOK, HEAD), jnp.bfloat16),
-            dma((13,)),
+            dma((11,)),
             dma((2,)),
-            dma((2, steps, 2, CHUNKS)),
+            dma((steps, 2, CHUNKS)),
             dma((2,)),
-            dma((2, zn)),
-            dma((2, CHUNKS)),
+            dma((zn,)),
+            dma((CHUNKS,)),
+            pltpu.SemaphoreType.REGULAR((2,)),
             dma,
             dma((steps,)),
             dma,
@@ -545,7 +541,7 @@
             dma((2, 2, 2)),
         ],
         compiler_params=pltpu.CompilerParams(
-            collective_id=0, has_side_effects=True, vmem_limit_bytes=67043328
+            collective_id=0, has_side_effects=True, vmem_limit_bytes=66777088
         ),
         name="neighbourhood",
     )(

time: 86.7 us -> 84 us (0.969)
  Pallas kernels: 85 us -> 83.2 us
  local copies, waits for them, and re-layouts: 1.57 us -> 0.66 us
    pallas_call x1, Pallas kernels: 85 us -> 83.2 us  [body(): pl.pallas_call(functools.partial(kernel, zn), out_shape=pltpu.VMEM((TOK,...]
    unnamed x1, local copies, waits for them, and re-layouts: 1.57 us -> 0.66 us
where the time goes in v5:
time: 84 us; the launch traced here: 83.9 us
  Pallas kernels  83.2 us (99%)
    pallas_call x1, Pallas kernels, body(): pl.pallas_call(functools.partial(kernel, zn), out_shape=pltpu.VMEM((TOK,...  83.2 us

profile of v5, /device:TPU:1, one launch (start us, length us, event | category | flops | bytes accessed | tf_op | source)
XLA Modules:
  0.0 83.9 jit_solution(5687270436931251551)
XLA Ops:
  0.0 83.2 %neighbourhood.1 = bf16[512,128]{1,0:T(8,128)(2,1)S(1)} custom-call(bf16[512,128]{1,0:T(8,128)(2,1)} %x_hbm.1, bf16[1,128]{1,0:T(2,128)(2,1)} %bitcast.18, bf16[1,128]{1,0:T(2,128)(2,1)} %bitcast.19, bf16[4,64,128]{2,1,0:T(8,128)(2,1)} %bitcast.10, bf16[4,64,128]{2,1,0:T(8,128)(2,1)} %bitcast.11, bf16[4,64,128]{2,1,0:T(8,128)(2,1)} %bitcast.12, ...), custom_call_target="tpu_custom_call" | custom-call | tf_op jit(solution)/shard_map/neighbourhood/pallas_call | solution.py:507
  83.2 0.7 copy.13

commit v6 on v5

--- a/solution.py
+++ b/solution.py
@@ -50,17 +50,17 @@
     (0, 4, 3): (("wait", 0, "1h"), ("send", 0, "2b"), ("wait", 0, "0b"), ("send", 0, "1b")),
     (0, 5, 1): (("wait", 0, "2a"), ("send", 0, "3")),
     (0, 6, 5): (("wait", 0, "3"), ("send", 1, "0a"), ("send", 1, "0b")),
-    (0, 8, 3): (("wait", 1, "0a"), ("send", 1, "1s")),
     (0, "halo", 0): (
-        ("wait", 1, "1s"),
-        ("send", 1, "2a"),
+        ("wait", 1, "0a"),
+        ("send", 1, "1s"),
         ("send", 1, "1h"),
         ("wait", 1, "0b"),
         ("send", 1, "1b"),
     ),
-    (1, 1, 5): (("wait", 1, "2a"), ("send", 1, "3")),
+    (1, 1, 5): (("wait", 1, "1s"), ("send", 1, "2a")),
     (1, 3, 1): (("wait", 1, "1h"), ("send", 1, "2b")),
-    (1, 5, 0): (("wait", 1, "3"),),
+    (1, 3, 4): (("wait", 1, "2a"), ("send", 1, "3")),
+    (1, 5, 1): (("wait", 1, "3"),),
 }
 BLOCKS_AT = {
     (0, 6, 6): (0,),

time: 84 us -> 84 us (level)
  no operation moved by 1% of the time
where the time goes in v6:
time: 84 us; the launch traced here: 83.9 us
  Pallas kernels  83.2 us (99%)
    pallas_call x1, Pallas kernels, body(): pl.pallas_call(functools.partial(kernel, zn), out_shape=pltpu.VMEM((TOK,...  83.2 us

profile of v6, /device:TPU:1, one launch (start us, length us, event | category | flops | bytes accessed | tf_op | source)
XLA Modules:
  0.0 83.9 jit_solution(14485287369091764483)
XLA Ops:
  0.0 83.2 %neighbourhood.1 = bf16[512,128]{1,0:T(8,128)(2,1)S(1)} custom-call(bf16[512,128]{1,0:T(8,128)(2,1)} %x_hbm.1, bf16[1,128]{1,0:T(2,128)(2,1)} %bitcast.18, bf16[1,128]{1,0:T(2,128)(2,1)} %bitcast.19, bf16[4,64,128]{2,1,0:T(8,128)(2,1)} %bitcast.10, bf16[4,64,128]{2,1,0:T(8,128)(2,1)} %bitcast.11, bf16[4,64,128]{2,1,0:T(8,128)(2,1)} %bitcast.12, ...), custom_call_target="tpu_custom_call" | custom-call | tf_op jit(solution)/shard_map/neighbourhood/pallas_call | solution.py:507
  83.2 0.7 copy.13
